TPU v7x, 32 devices: a whole 2x2x4 slice. The times are simulated.
32 devices in a mesh: sp: 16 (over z, y, x), tp: 2 (over core).
Axes of the slice: x: 2, y: 2, z: 4, core: 2. Of those that a mesh axis runs over, the one named last changes fastest.
Arguments:
- normed: bfloat16 [4096, 2048], P(('sp', 'tp')), may hold values from -40 to 40
- query_weight: bfloat16 [2048, 2048], P(None, 'tp'), may hold values from -1.5 to 1.5
- key_weight: bfloat16 [2048, 2048], P(None, 'tp'), may hold values from -1 to 1
- value_weight: bfloat16 [2048, 2048], P(None, 'tp'), may hold values from -0.125 to 0.125
- pool_in_weight: bfloat16 [2048, 1024], P(None, 'tp'), may hold values from -0.125 to 0.125
- pool_weight: bfloat16 [8, 128, 128], P('tp'), may hold values from -0.5 to 0.5
- map_balance: float32 [8], replicated, may hold values from 0.3 to 0.8
- head_gain: float32 [256], replicated, may hold values from 0.1 to 1.9
- contrast_out_weight: bfloat16 [2048, 2048], P('tp'), may hold values from -0.109375 to 0.109375
- pool_out_weight: bfloat16 [1024, 2048], P('tp'), may hold values from -0.109375 to 0.109375
Outputs:
- layer_out: bfloat16 [4096, 2048], P(('sp', 'tp'))
All inputs are finite; a program needn't handle non-finite values.
Results may differ from a plain program's by a relative error of at most 0.03.
Values may be sent and summed in bfloat16 or wider, within the bound.
No kernel may reach another device: no remote copies, remote signals or barrier semaphores. Data moves between devices by JAX's collectives and lax.ppermute only.
A program may use at most 128 MiB of HBM per device.

v0:
```python
import math

import jax
import jax.numpy as jnp
from jax import lax
from jax.sharding import PartitionSpec as P

reach_back = 15
norm_epsilon = 1e-06


def passed_along(block, axis, distance):
    devices = range(lax.axis_size(axis))
    route = [(i - distance, i) for i in devices if i - distance in devices]
    return lax.ppermute(block, axis, route)


def from_partner(block, axis, stride):
    count = lax.axis_size(axis)
    route = []
    for low in range(count):
        high = low | 1 << stride
        if high != low and high < count:
            route += [(low, high), (high, low)]
    return lax.ppermute(block, axis, route)


def shifted(array, axis, by):
    size = lax.axis_size(axis)
    return lax.ppermute(array, axis, [(i, (i + by) % size) for i in range(size)])


def as_sent(array):

    def short(part):
        return part.astype(jnp.bfloat16) if part.dtype == jnp.float32 else part

    return jax.tree.map(short, array)


def attend(running, queries, key_rows, value_rows, query_first, key_first, score_scale):
    key_count = key_rows.shape[0]
    key_block = math.gcd(key_count, 1024)
    unit_count = queries.shape[1]
    heads_here = value_rows.shape[1]
    per_head = unit_count // heads_here
    query_count = queries.shape[0]
    query_order = query_first + lax.iota(jnp.int32, query_count)

    def key_step(block_index, carried):
        block_start = block_index * key_block

        def block_work(current):
            row_peak, row_total, weighted = current
            scores = (
                jnp.einsum("qud,kud->uqk", queries, key_rows, preferred_element_type=jnp.float32)
                * score_scale
            )
            key_order = key_first + block_start + lax.iota(jnp.int32, key_block)
            scores = jnp.where(
                key_order[None, None, :] <= query_order[None, :, None], scores, -jnp.inf
            )
            new_peak = jnp.maximum(row_peak, jnp.max(scores, axis=2))
            shrink = jnp.exp(row_peak - new_peak)
            raised = jnp.exp(scores - new_peak[:, :, None])
            row_total = row_total * shrink + jnp.sum(raised, axis=2)
            map_weights = raised.astype(jnp.bfloat16).reshape(
                heads_here, per_head, query_count, key_block
            )
            update = jnp.einsum(
                "hmqk,khe->hmqe", map_weights, value_rows, preferred_element_type=jnp.float32
            )
            weighted = weighted * shrink[:, :, None] + update.reshape(unit_count, query_count, -1)
            return (new_peak, row_total, weighted)

        def keep_state(current):
            return current

        return lax.cond(
            key_first + block_start <= query_first + query_count - 1,
            block_work,
            keep_state,
            carried,
        )

    return lax.fori_loop(0, key_count // key_block, key_step, running)


def fresh_state(unit_count, row_count, value_width):
    return (
        jnp.full((unit_count, row_count), -1e30, jnp.float32),
        jnp.zeros((unit_count, row_count), jnp.float32),
        jnp.zeros((unit_count, row_count, value_width), jnp.float32),
    )


def finished(running):
    row_peak, row_total, weighted = running
    return (weighted / row_total[:, :, None]).astype(jnp.bfloat16)


def joined_state(first, second):
    first_peak, first_total, first_weighted = first
    second_peak, second_total, second_weighted = second
    new_peak = jnp.maximum(first_peak, second_peak)
    first_shrink = jnp.exp(first_peak - new_peak)
    second_shrink = jnp.exp(second_peak - new_peak)
    new_total = first_total * first_shrink + second_total * second_shrink
    new_weighted = (
        first_weighted * first_shrink[:, :, None] + second_weighted * second_shrink[:, :, None]
    )
    return (new_peak, new_total, new_weighted)


def per_device(
    normed,
    query_weight,
    key_weight,
    value_weight,
    pool_in_weight,
    pool_weight,
    map_balance,
    head_gain,
    contrast_out_weight,
    pool_out_weight,
):
    tp_index = lax.axis_index("tp")
    sp_count = lax.axis_size("sp")
    sp_index = lax.axis_index("sp")
    head_dim = head_gain.shape[0] // 2
    value_width = 2 * head_dim
    query_cols = query_weight.shape[1]
    value_cols = value_weight.shape[1]
    unit_count = query_cols // head_dim
    heads_here = unit_count // 2
    project_incoming = lax.all_gather(normed, "tp", axis=0, tiled=True)
    products = [
        jnp.dot(project_incoming, weight_part, preferred_element_type=jnp.float32)
        for weight_part in (query_weight, key_weight, value_weight, pool_in_weight)
    ]
    joined = jnp.concatenate(products, axis=1).astype(jnp.bfloat16)
    row_count = joined.shape[0]
    queries = joined[:, :query_cols].reshape(row_count, unit_count, head_dim)
    key_rows = joined[:, query_cols : 2 * query_cols].reshape(row_count, unit_count, head_dim)
    value_rows = joined[:, 2 * query_cols : 2 * query_cols + value_cols].reshape(
        row_count, heads_here, value_width
    )
    pool_input = joined[:, 2 * query_cols + value_cols :]
    pool_cols = pool_input.shape[1]
    upper_rim = passed_along(pool_input[row_count - reach_back :], "sp", 1)
    extended = jnp.concatenate([upper_rim, pool_input], axis=0).astype(jnp.float32)
    groups_here = pool_weight.shape[0]
    group_width = pool_weight.shape[1]
    group_index = tp_index * groups_here + lax.iota(jnp.int32, pool_cols) // group_width
    widths = jnp.left_shift(jnp.int32(2), group_index % 4)
    window_sum = jnp.zeros((row_count, pool_cols), jnp.float32)
    for offset in range(reach_back + 1):
        window_sum = window_sum + extended[
            reach_back - offset : reach_back - offset + row_count
        ] * (offset < widths)[None, :].astype(jnp.float32)
    position = sp_index * row_count + lax.iota(jnp.int32, row_count)
    counts = jnp.minimum(position[:, None] + 1, widths[None, :]).astype(jnp.float32)
    spread = (window_sum / counts - extended[reach_back:]).astype(jnp.bfloat16)
    mixed_groups = jnp.einsum(
        "tgc,gce->tge",
        spread.reshape(row_count, groups_here, group_width),
        pool_weight,
        preferred_element_type=jnp.float32,
    )
    pool_out = mixed_groups.reshape(row_count, pool_cols).astype(jnp.bfloat16)
    score_scale = head_dim ** (-0.5)
    level_count = sp_count.bit_length() - 1
    low_levels = level_count // 2
    band_size = 1 << low_levels
    band_count = sp_count // band_size
    member = sp_index % band_size
    band = sp_index // band_size
    band_queries = queries
    for bit in range(low_levels):
        received = from_partner(band_queries, "sp", bit)
        upper = member >> bit & 1 == 1
        band_queries = jnp.where(
            upper,
            jnp.concatenate([received, band_queries], axis=0),
            jnp.concatenate([band_queries, received], axis=0),
        )
    band_first = band * band_size * row_count
    running = fresh_state(unit_count, band_size * row_count, value_width)
    for step in range(band_count):
        if step == 0:
            key_piece, value_piece = (key_rows, value_rows)
        else:
            key_piece, value_piece = shifted((key_rows, value_rows), "sp", step * band_size)
        source = (sp_index - step * band_size) % sp_count
        running = attend(
            running,
            band_queries,
            key_piece,
            value_piece,
            band_first,
            source * row_count,
            score_scale,
        )
    for bit in range(low_levels - 1, -1, -1):
        half = running[0].shape[1] // 2
        upper = member >> bit & 1 == 1
        lower_part = jax.tree.map(lambda item: item[:, :half], running)
        upper_part = jax.tree.map(lambda item: item[:, half:], running)
        outgoing = jax.tree.map(
            lambda low, high: jnp.where(upper, low, high), lower_part, upper_part
        )
        kept = jax.tree.map(lambda low, high: jnp.where(upper, high, low), lower_part, upper_part)
        incoming = from_partner(
            (as_sent(outgoing[0]), as_sent(outgoing[1]), as_sent(outgoing[2])), "sp", bit
        )
        running = joined_state(kept, incoming)
    maps = finished(running)
    paired = maps.reshape(heads_here, 2, row_count, value_width)
    paired = lax.optimization_barrier(paired).astype(jnp.float32)
    head_first = tp_index * heads_here
    balance_here = lax.dynamic_slice_in_dim(map_balance, head_first, heads_here, 0)
    contrast = paired[:, 0] - balance_here[:, None, None] * paired[:, 1]
    mean_square = jnp.mean(contrast * contrast, axis=2, keepdims=True)
    contrast = contrast * lax.rsqrt(mean_square + norm_epsilon) * head_gain
    contrast_out = (
        contrast.astype(jnp.bfloat16)
        .transpose(1, 0, 2)
        .reshape(row_count, heads_here * value_width)
    )
    partial_value = jnp.dot(contrast_out, contrast_out_weight, preferred_element_type=jnp.float32)
    return lax.psum_scatter(
        (
            partial_value + jnp.dot(pool_out, pool_out_weight, preferred_element_type=jnp.float32)
        ).astype(jnp.bfloat16),
        "tp",
        scatter_dimension=0,
        tiled=True,
    )


def solution(mesh):
    return jax.shard_map(
        per_device,
        mesh=mesh,
        in_specs=(
            P(("sp", "tp"), None),
            P(None, "tp"),
            P(None, "tp"),
            P(None, "tp"),
            P(None, "tp"),
            P("tp", None, None),
            P(),
            P(),
            P("tp", None),
            P("tp", None),
        ),
        out_specs=P(("sp", "tp"), None),
        check_vma=False,
    )
```

profile of v0, /device:TPU:17, one launch (start us, length us, event | category | flops | bytes accessed | tf_op | source)
XLA Modules:
  0.0 269.4 jit_solution(1094205833064472675)
XLA Ops:
  6.5 0.7 all-gather.2.cloned.1.call-update
  7.3 12.4 %all-gather.2.cloned.1.call-done = bf16[256,2048]{1,0:T(8,128)(2,1)} async-done(((bf16[128,2048]{1,0:T(8,128)(2,1)}), bf16[256,2048]{1,0:T(8,128)(2,1)}) %all-gather.2.cloned.1.call-update) | async-done | bytes 1048592 | tf_op jit(solution)/shard_map/all_gather | solution.py:136
  19.7 3.8 %fusion.23 = bf16[32,8,8,128]{3,2,1,0:T(8,128)(2,1)S(1)} fusion(bf16[256,2048]{1,0:T(8,128)(2,1)} %all-gather.2.cloned.1.call-done, bf16[2048,1024]{1,0:T(8,128)(2,1)} %param.19), kind=kOutput, calls=%fused_computation.60 | convolution fusion | flops 1074003968 | bytes 5767168 | tf_op jit(solution)/shard_map/dot_general | solution.py:138
  23.6 1.3 collective-permute-start
  24.9 12.2 %collective-permute-done = bf16[256,8,128]{2,0,1:T(8,128)(2,1)} collective-permute-done((bf16[256,8,128]{2,0,1:T(8,128)(2,1)S(1)}, bf16[256,8,128]{2,0,1:T(8,128)(2,1)}, u32[]{:S(2)}, u32[]{:S(2)}) %collective-permute-start) | collective-permute-done | bytes 524320 | tf_op jit(solution)/shard_map/ppermute | solution.py:25
  37.0 1.9 maximum_select_fusion.1
  38.9 1.3 collective-permute-start.1
  40.2 4.0 %convolution_convert_fusion.1 = bf16[256,1024]{1,0:T(8,128)(2,1)S(1)} fusion(bf16[256,2048]{1,0:T(8,128)(2,1)} %all-gather.2.cloned.1.call-done, bf16[2048,1024]{1,0:T(8,128)(2,1)} %param.20), kind=kOutput, calls=%fused_computation.58 | convolution fusion | flops 1074003968 | bytes 5767168 | tf_op jit(solution)/shard_map/dot_general | solution.py:138
  44.3 1.0 copy_bitcast_fusion.1
  45.2 1.2 collective-permute-start.2
  46.5 1.3 convolution_convert_fusion
  47.8 0.9 copy.95
  48.6 1.4 collective-permute-start.4
  50.1 0.9 collective-permute-start.5
  51.0 6.8 %collective-permute-done.2 = bf16[256,8,128]{2,0,1:T(8,128)(2,1)S(1)} collective-permute-done((bf16[256,8,128]{2,0,1:T(8,128)(2,1)}, bf16[256,8,128]{2,0,1:T(8,128)(2,1)S(1)}, u32[]{:S(2)}, u32[]{:S(2)}) %collective-permute-start.2) | collective-permute-done | bytes 524320 | tf_op jit(solution)/shard_map/ppermute | solution.py:30
  57.8 0.3 collective-permute-start.6
  58.1 4.7 %collective-permute-done.1 = bf16[512,8,128]{2,0,1:T(8,128)(2,1)S(1)} collective-permute-done((bf16[512,8,128]{2,0,1:T(8,128)(2,1)S(1)}, bf16[512,8,128]{2,0,1:T(8,128)(2,1)S(1)}, u32[]{:S(2)}, u32[]{:S(2)}) %collective-permute-start.1) | collective-permute-done | bytes 1048608 | tf_op jit(solution)/shard_map/ppermute | solution.py:25
  62.8 1.0 copy-done.5
  63.8 0.3 collective-permute-start.7
  64.1 4.0 %broadcast_in_dim.65 = f32[8,1024,256]{2,1,0:T(8,128)} broadcast(f32[]{:T(128)} %constant.213.clone.1), dimensions={} | broadcast | bytes 8388612 | tf_op jit(solution)/shard_map/broadcast_in_dim | solution.py:93
  68.1 2.2 reshape.326
  70.4 1.9 copy.81
  72.3 3.5 %maximum_select_fusion = bf16[1024,8,128]{2,0,1:T(8,128)(2,1)} fusion(bf16[512,8,128]{2,0,1:T(8,128)(2,1)S(1)} %maximum_select_fusion.1, bf16[512,8,128]{2,0,1:T(8,128)(2,1)} %copy-done.5, pred[]{:T(512)S(6)} %eq.17), kind=kLoop, calls=%fused_computation.54 | loop fusion | flops 9437184 | bytes 4194305 | tf_op jit(solution)/shard_map/jit(_where)/select_n | solution.py:182
  75.8 13.8 %conditional.4 = ((f32[8,1024]{1,0:T(8,128)S(1)}, f32[8,1024]{1,0:T(8,128)S(1)}, f32[8,1024,256]{2,1,0:T(8,128)})) conditional(s32[]{:T(128)} %convert_element_type.230, (f32[8,1024]{1,0:T(8,128)S(1)}, f32[8,1024]{1,0:T(8,128)S(1)}, f32[8,1024,256]{2,1,0:T(8,128)}) %tuple.64, (s32[]{:T(128)}, s32[1024]{0:T(1024)S(1)}, ...), branch_computations={%region_0.1_spmd, %region_1.4_spmd} | conditional | flops 1631863040 | bytes 65247296 | solution.py:79
  75.8 0.2 broadcast_compare_fusion
  76.1 3.2 %fusion = (f32[8,1024]{1,0:T(8,128)S(1)}, f32[8,1024,256]{1,2,0:T(8,128)S(1)}) fusion(pred[1024,256]{0,1:T(8,128)(4,1)S(1)} %broadcast_compare_fusion, bf16[1024,8,128]{2,0,1:T(8,128)(2,1)} %get-tuple-element.304, bf16[256,8,128]{2,1,0:T(8,128)(2,1)} %get-tuple-element.408), kind=kOutput, calls=%fused_computation.3 | convolution fusion | flops 543154176 | bytes 11304960 | tf_op jit(solution)/shard_map/while/body/eval_jaxpr/cond/branch_1_fun/qud,kud->uqk/dot_general | solution.py:56
  79.3 2.0 fusion.1
  81.4 1.8 fusion.3
  83.2 6.4 %bitcast_add_fusion = f32[8,1024,256]{2,1,0:T(8,128)} fusion(f32[4,2,1024,256]{3,2,1,0:T(8,128)S(1)} %fusion.3, f32[8,1024,256]{2,1,0:T(8,128)} %get-tuple-element.307, f32[8,1024]{1,0:T(8,128)S(1)} %get-tuple-element.417), kind=kLoop, calls=%fused_computation | loop fusion | flops 4194304 | bytes 25198592 | tf_op jit(solution)/shard_map/while/body/eval_jaxpr/cond/branch_1_fun/add | solution.py:73
  89.6 14.8 %conditional.5 = ((f32[8,1024]{1,0:T(8,128)S(1)}, f32[8,1024]{1,0:T(8,128)S(1)}, f32[8,1024,256]{2,1,0:T(8,128)})) conditional(s32[]{:T(128)} %convert_element_type.229, (f32[8,1024]{1,0:T(8,128)S(1)}, f32[8,1024]{1,0:T(8,128)S(1)}, f32[8,1024,256]{2,1,0:T(8,128)}) %get-tuple-element.487, (s32[]{:T(128)}, s32[1024]{0:T(1024)S(1)}, ...), branch_computations={%region_4.5_spmd, %region_5.8_spmd} | conditional | flops 1631863040 | bytes 63150116 | solution.py:79
  89.8 0.2 broadcast_compare_fusion.1
  90.0 3.0 %fusion.7 = (f32[8,1024]{1,0:T(8,128)S(1)}, f32[8,1024,256]{1,2,0:T(8,128)S(1)}) fusion(pred[1024,256]{0,1:T(8,128)(4,1)S(1)} %broadcast_compare_fusion.1, bf16[1024,8,128]{2,0,1:T(8,128)(2,1)} %get-tuple-element.312, bf16[256,8,128]{2,0,1:T(8,128)(2,1)S(1)} %get-tuple-element.313), kind=kOutput, calls=%fused_computation.17 | convolution fusion | flops 543154176 | bytes 11304960 | tf_op jit(solution)/shard_map/while/body/eval_jaxpr/cond/branch_1_fun/qud,kud->uqk/dot_general | solution.py:56
  93.1 2.0 fusion.8
  95.2 2.8 %fusion.10 = f32[4,2,1024,256]{3,2,1,0:T(8,128)S(1)} fusion(bf16[4,2,1024,256]{2,3,1,0:T(8,128)(2,1)S(1)} %bitcast.103, bf16[256,4,256]{2,0,1:T(8,128)(2,1)} %get-tuple-element.316), kind=kOutput, calls=%fused_computation.20 | convolution fusion | flops 1073741824 | bytes 13107200 | tf_op jit(solution)/shard_map/while/body/eval_jaxpr/cond/branch_1_fun/hmqk,khe->hmqe/dot_general | solution.py:70
  98.0 6.4 %bitcast_add_fusion.1 = f32[8,1024,256]{2,1,0:T(8,128)} fusion(f32[4,2,1024,256]{3,2,1,0:T(8,128)S(1)} %fusion.10, f32[8,1024,256]{2,1,0:T(8,128)} %get-tuple-element.315, f32[8,1024]{1,0:T(8,128)S(1)} %get-tuple-element.419), kind=kLoop, calls=%fused_computation.14 | loop fusion | flops 4194304 | bytes 25198592 | tf_op jit(solution)/shard_map/while/body/eval_jaxpr/cond/branch_1_fun/add | solution.py:73
  104.4 9.9 %collective-permute-done.5 = bf16[256,4,256]{2,0,1:T(8,128)(2,1)} collective-permute-done((bf16[256,4,256]{2,0,1:T(8,128)(2,1)}, bf16[256,4,256]{2,0,1:T(8,128)(2,1)}, u32[]{:S(2)}, u32[]{:S(2)}) %collective-permute-start.5) | collective-permute-done | bytes 524320 | tf_op jit(solution)/shard_map/ppermute | solution.py:30
  114.4 14.7 %conditional.6 = ((f32[8,1024]{1,0:T(8,128)S(1)}, f32[8,1024]{1,0:T(8,128)S(1)}, f32[8,1024,256]{2,1,0:T(8,128)})) conditional(s32[]{:T(128)} %convert_element_type.228, (f32[8,1024]{1,0:T(8,128)S(1)}, f32[8,1024]{1,0:T(8,128)S(1)}, f32[8,1024,256]{2,1,0:T(8,128)}) %get-tuple-element.488, (s32[]{:T(128)}, s32[1024]{0:T(1024)S(1)}, ...), branch_computations={%region_8.9_spmd, %region_9.12_spmd} | conditional | flops 1631863040 | bytes 63150116 | solution.py:79
  114.4 0.2 broadcast_compare_fusion.2
  114.6 3.1 %fusion.12 = (f32[8,1024]{1,0:T(8,128)S(1)}, f32[8,1024,256]{1,2,0:T(8,128)S(1)}) fusion(pred[1024,256]{0,1:T(8,128)(4,1)S(1)} %broadcast_compare_fusion.2, bf16[1024,8,128]{2,0,1:T(8,128)(2,1)} %get-tuple-element.320, bf16[256,8,128]{2,0,1:T(8,128)(2,1)} %get-tuple-element.321), kind=kOutput, calls=%fused_computation.29 | convolution fusion | flops 543154176 | bytes 11304960 | tf_op jit(solution)/shard_map/while/body/eval_jaxpr/cond/branch_1_fun/qud,kud->uqk/dot_general | solution.py:56
  117.7 2.0 fusion.13
  119.8 2.8 %fusion.15 = f32[4,2,1024,256]{3,2,1,0:T(8,128)S(1)} fusion(bf16[4,2,1024,256]{2,3,1,0:T(8,128)(2,1)S(1)} %bitcast.104, bf16[256,4,256]{2,0,1:T(8,128)(2,1)} %get-tuple-element.324), kind=kOutput, calls=%fused_computation.32 | convolution fusion | flops 1073741824 | bytes 13107200 | tf_op jit(solution)/shard_map/while/body/eval_jaxpr/cond/branch_1_fun/hmqk,khe->hmqe/dot_general | solution.py:70
  122.6 6.4 %bitcast_add_fusion.2 = f32[8,1024,256]{2,1,0:T(8,128)} fusion(f32[4,2,1024,256]{3,2,1,0:T(8,128)S(1)} %fusion.15, f32[8,1024,256]{2,1,0:T(8,128)} %get-tuple-element.323, f32[8,1024]{1,0:T(8,128)S(1)} %get-tuple-element.421), kind=kLoop, calls=%fused_computation.26 | loop fusion | flops 4194304 | bytes 25198592 | tf_op jit(solution)/shard_map/while/body/eval_jaxpr/cond/branch_1_fun/add | solution.py:73
  129.1 7.8 %collective-permute-done.7 = bf16[256,4,256]{2,0,1:T(8,128)(2,1)} collective-permute-done((bf16[256,4,256]{2,0,1:T(8,128)(2,1)}, bf16[256,4,256]{2,0,1:T(8,128)(2,1)}, u32[]{:S(2)}, u32[]{:S(2)}) %collective-permute-start.7) | collective-permute-done | bytes 524320 | tf_op jit(solution)/shard_map/ppermute | solution.py:30
  136.8 4.0 %select_convert_fusion = bf16[8,512,256]{2,1,0:T(8,128)(2,1)S(1)} fusion(f32[8,1024,256]{2,1,0:T(8,128)} %get-tuple-element.413, pred[]{:T(512)S(6)} %eq.17), kind=kLoop, calls=%fused_computation.51 | loop fusion | flops 1048576 | bytes 6291457 | tf_op jit(solution)/shard_map/convert_element_type | solution.py:36
  140.8 0.2 collective-permute-start.9
  141.2 0.7 convolution_convert_fusion.4
  141.9 3.3 %collective-permute-start.14 = (bf16[15,512]{1,0:T(8,128)(2,1)S(1)}, bf16[15,512]{1,0:T(8,128)(2,1)S(1)}, u32[]{:S(2)}, u32[]{:S(2)}) collective-permute-start(bf16[15,512]{1,0:T(8,128)(2,1)S(1)} %slice.241), channel_id=1, source_target_pairs={{0,2},{2,4},{4,6},{6,8},{8,10},{10,12},{12,14},{14,16},{16,18},{18... | collective-permute-start | bytes 46088 | tf_op jit(solution)/shard_map/ppermute | solution.py:15
  145.2 1.4 collective-permute-start.12
  146.8 2.6 collective-permute-done.14
  149.5 28.8 %collective-permute-done.12 = bf16[8,512]{1,0:T(8,128)(2,1)S(1)} collective-permute-done((bf16[8,512]{1,0:T(8,128)(2,1)S(1)}, bf16[8,512]{1,0:T(8,128)(2,1)S(1)}, u32[]{:S(2)}, u32[]{:S(2)}) %collective-permute-start.12) | collective-permute-done | bytes 8224 | tf_op jit(solution)/shard_map/ppermute | solution.py:25
  178.5 4.7 %multiply_add_fusion.4 = f32[8,512,256]{2,1,0:T(8,128)S(1)} fusion(bf16[8,512,256]{2,1,0:T(8,128)(2,1)S(1)} %collective-permute-done.9, f32[8,1024,256]{2,1,0:T(8,128)} %get-tuple-element.413, f32[8,512]{1,0:T(8,128)S(1)} %get-tuple-element.429, f32[8,512]{1,0:T(8,128)S(1)} %get-tuple-element.428, pred[]{:T(512)S(6)} %eq.17), kind=kLoop, calls=%fused_computation.50 | loop fusion | flops 5242880 | bytes 14712833 | tf_op jit(solution)/shard_map/add | solution.py:110
  183.2 0.2 select_convert_fusion.1
  183.4 1.3 collective-permute-start.11
  184.7 0.2 collective-permute-start.13
  184.9 1.2 collective-permute-start.10
  186.2 1.3 convolution_convert_fusion.3
  187.5 9.7 %collective-permute-done.13 = bf16[8,256]{1,0:T(8,128)(2,1)S(1)} collective-permute-done((bf16[8,256]{1,0:T(8,128)(2,1)S(1)}, bf16[8,256]{1,0:T(8,128)(2,1)S(1)}, u32[]{:S(2)}, u32[]{:S(2)}) %collective-permute-start.13) | collective-permute-done | bytes 4128 | tf_op jit(solution)/shard_map/ppermute | solution.py:25
  197.2 1.0 divide_convert_fusion
  198.4 0.3 multiply_reduce_fusion
  198.9 0.2 fusion.26
  199.2 0.2 copy.62
  199.4 3.5 %fusion.60 = f32[256,2048]{1,0:T(8,128)S(1)} fusion(bf16[256,1024]{0,1:T(8,128)(2,1)S(1)} %bitcast.113, bf16[1024,2048]{1,0:T(8,128)(2,1)} %param.26), kind=kOutput, calls=%fused_computation.159 | convolution fusion | flops 1073741824 | bytes 6815744 | tf_op jit(solution)/shard_map/dot_general | solution.py:230
  202.8 1.7 fusion.22
  204.6 58.0 %reduce-scatter.2.cloned.1.call-done = bf16[128,2048]{1,0:T(8,128)(2,1)} async-done(((bf16[256,2048]{1,0:T(8,128)(2,1)}), bf16[128,2048]{1,0:T(8,128)(2,1)}) %reduce-scatter.2.cloned.1.call-update) | async-done | bytes 524304 | tf_op jit(solution)/shard_map/reduce_scatter | solution.py:231
  (79 shorter events, 1.4 us)
Async XLA Ops:
  6.5 196.3 %copy-start = (bf16[512,2048]{1,0:T(8,128)(2,1)S(1)}, bf16[512,2048]{1,0:T(8,128)(2,1)}, u32[]{:S(2)}) copy-start(bf16[512,2048]{1,0:T(8,128)(2,1)} %param.27) | copy-start | bytes 6291460
  6.5 13.2 %all-gather.2.cloned.1.call-start = ((), (), s32[]{:S(2)}) async-start(), calls=%async_computation.1 | async-start | bytes 1572864 | tf_op jit(solution)/shard_map/all_gather | solution.py:136
  7.3 255.3 %reduce-scatter.2.cloned.1.call-start = ((), (), s32[]{:S(2)}) async-start(), calls=%async_computation.2 | async-start | bytes 1572864 | tf_op jit(solution)/shard_map/reduce_scatter | solution.py:231
  23.6 1.3 copy-start.2
  23.6 13.4 %collective-permute-start = (bf16[256,8,128]{2,0,1:T(8,128)(2,1)S(1)}, bf16[256,8,128]{2,0,1:T(8,128)(2,1)}, u32[]{:S(2)}, u32[]{:S(2)}) collective-permute-start(bf16[256,8,128]{2,0,1:T(8,128)(2,1)S(1)} %bitcast.109), channel_id=1, source_target_pairs={{0,2},{2,0},{4,6},{6,4},{8,10},{10,8},{12,14},{14,12},{16,18},{18,... | collective-permute-start | bytes 1572872 | tf_op jit(solution)/shard_map/ppermute | solution.py:25
  38.9 7.5 %copy-start.9 = (bf16[2048,1024]{1,0:T(8,128)(2,1)S(1)}, bf16[2048,1024]{1,0:T(8,128)(2,1)}, u32[]{:S(2)}) copy-start(bf16[2048,1024]{1,0:T(8,128)(2,1)} %param.21) | copy-start | bytes 12582916
  38.9 7.5 %copy-start.11 = (bf16[256,2048]{1,0:T(8,128)(2,1)S(1)}, bf16[256,2048]{1,0:T(8,128)(2,1)}, u32[]{:S(2)}) copy-start(bf16[256,2048]{1,0:T(8,128)(2,1)} %all-gather.2.cloned.1.call-done) | copy-start | bytes 3145732
  38.9 23.8 %collective-permute-start.1 = (bf16[512,8,128]{2,0,1:T(8,128)(2,1)S(1)}, bf16[512,8,128]{2,0,1:T(8,128)(2,1)S(1)}, u32[]{:S(2)}, u32[]{:S(2)}) collective-permute-start(bf16[512,8,128]{2,0,1:T(8,128)(2,1)S(1)} %maximum_select_fusion.1), channel_id=1, source_target_pairs={{0,4},{4,0},{2,6},{6,2},{8,12},{12,8},{10,14},{14,10},{16,20},{20,... | collective-permute-start | bytes 3145736 | tf_op jit(solution)/shard_map/ppermute | solution.py:25
  44.3 3.5 %copy-start.3 = (bf16[256,1024]{1,0:T(8,128)(2,1)}, bf16[256,1024]{1,0:T(8,128)(2,1)S(1)}, u32[]{:S(2)}) copy-start(bf16[256,1024]{1,0:T(8,128)(2,1)S(1)} %convolution_convert_fusion.1) | copy-start | bytes 1572868
  45.2 18.8 %copy-start.14 = (f32[8]{0:T(128)S(1)}, f32[8]{0:T(128)}, u32[]{:S(2)}) copy-start(f32[8]{0:T(128)} %param.24) | copy-start | bytes 100
  45.2 12.6 %collective-permute-start.2 = (bf16[256,8,128]{2,0,1:T(8,128)(2,1)}, bf16[256,8,128]{2,0,1:T(8,128)(2,1)S(1)}, u32[]{:S(2)}, u32[]{:S(2)}) collective-permute-start(bf16[256,8,128]{2,0,1:T(8,128)(2,1)} %copy_bitcast_fusion.1), channel_id=1, source_target_pairs={{0,8},{2,10},{4,12},{6,14},{8,16},{10,18},{12,20},{14,22},{16,24},... | collective-permute-start | bytes 1572872 | tf_op jit(solution)/shard_map/ppermute | solution.py:30
  47.7 15.0 %copy-start.4 = (bf16[256,1024]{1,0:T(8,128)(2,1)}, bf16[256,1024]{1,0:T(8,128)(2,1)S(1)}, u32[]{:S(2)}) copy-start(bf16[256,1024]{1,0:T(8,128)(2,1)S(1)} %convolution_convert_fusion) | copy-start | bytes 1572868
  48.6 41.0 %collective-permute-start.3 = (bf16[256,4,256]{2,0,1:T(8,128)(2,1)}, bf16[256,4,256]{2,0,1:T(8,128)(2,1)}, u32[]{:S(2)}, u32[]{:S(2)}) collective-permute-start(bf16[256,4,256]{2,0,1:T(8,128)(2,1)} %bitcast.100), channel_id=1, source_target_pairs={{0,8},{2,10},{4,12},{6,14},{8,16},{10,18},{12,20},{14,22},{16,24},... | collective-permute-start | bytes 1572872 | tf_op jit(solution)/shard_map/ppermute | solution.py:30
  48.6 55.8 %collective-permute-start.4 = (bf16[256,8,128]{2,0,1:T(8,128)(2,1)}, bf16[256,8,128]{2,0,1:T(8,128)(2,1)}, u32[]{:S(2)}, u32[]{:S(2)}) collective-permute-start(bf16[256,8,128]{2,0,1:T(8,128)(2,1)} %copy_bitcast_fusion.1), channel_id=1, source_target_pairs={{0,16},{2,18},{4,20},{6,22},{8,24},{10,26},{12,28},{14,30},{16,0},... | collective-permute-start | bytes 1572872 | tf_op jit(solution)/shard_map/ppermute | solution.py:30
  50.1 64.3 %collective-permute-start.5 = (bf16[256,4,256]{2,0,1:T(8,128)(2,1)}, bf16[256,4,256]{2,0,1:T(8,128)(2,1)}, u32[]{:S(2)}, u32[]{:S(2)}) collective-permute-start(bf16[256,4,256]{2,0,1:T(8,128)(2,1)} %bitcast.100), channel_id=1, source_target_pairs={{0,16},{2,18},{4,20},{6,22},{8,24},{10,26},{12,28},{14,30},{16,0},... | collective-permute-start | bytes 1572872 | tf_op jit(solution)/shard_map/ppermute | solution.py:30
  57.8 4.9 %copy-start.6 = (bf16[256,8,128]{2,0,1:T(8,128)(2,1)}, bf16[256,8,128]{2,0,1:T(8,128)(2,1)S(1)}, u32[]{:S(2)}) copy-start(bf16[256,8,128]{2,0,1:T(8,128)(2,1)S(1)} %collective-permute-done.2) | copy-start | bytes 1572868
  57.8 71.2 %collective-permute-start.6 = (bf16[256,8,128]{2,0,1:T(8,128)(2,1)}, bf16[256,8,128]{2,0,1:T(8,128)(2,1)}, u32[]{:S(2)}, u32[]{:S(2)}) collective-permute-start(bf16[256,8,128]{2,0,1:T(8,128)(2,1)} %copy_bitcast_fusion.1), channel_id=1, source_target_pairs={{0,24},{2,26},{4,28},{6,30},{8,0},{10,2},{12,4},{14,6},{16,8},{18,... | collective-permute-start | bytes 1572872 | tf_op jit(solution)/shard_map/ppermute | solution.py:30
  62.8 1.0 copy-start.5
  63.8 73.0 %collective-permute-start.7 = (bf16[256,4,256]{2,0,1:T(8,128)(2,1)}, bf16[256,4,256]{2,0,1:T(8,128)(2,1)}, u32[]{:S(2)}, u32[]{:S(2)}) collective-permute-start(bf16[256,4,256]{2,0,1:T(8,128)(2,1)} %bitcast.100), channel_id=1, source_target_pairs={{0,24},{2,26},{4,28},{6,30},{8,0},{10,2},{12,4},{14,6},{16,8},{18,... | collective-permute-start | bytes 1572872 | tf_op jit(solution)/shard_map/ppermute | solution.py:30
  75.8 13.8 %copy-start.7 = (bf16[256,8,128]{2,0,1:T(8,128)(2,1)S(1)}, bf16[256,8,128]{2,0,1:T(8,128)(2,1)}, u32[]{:S(2)}) copy-start(bf16[256,8,128]{2,0,1:T(8,128)(2,1)} %copy-done.6) | copy-start | bytes 1572868
  79.3 2.1 copy-start.1
  136.8 4.3 %copy-start.10 = (bf16[2048,512]{1,0:T(8,128)(2,1)S(1)}, bf16[2048,512]{1,0:T(8,128)(2,1)}, u32[]{:S(2)}) copy-start(bf16[2048,512]{1,0:T(8,128)(2,1)} %param.22) | copy-start | bytes 6291460
  136.8 4.3 %copy-start.12 = (bf16[256,2048]{1,0:T(8,128)(2,1)S(1)}, bf16[256,2048]{1,0:T(8,128)(2,1)}, u32[]{:S(2)}) copy-start(bf16[256,2048]{1,0:T(8,128)(2,1)} %all-gather.2.cloned.1.call-done) | copy-start | bytes 3145732
  140.8 37.7 %collective-permute-start.9 = (bf16[8,512,256]{2,1,0:T(8,128)(2,1)S(1)}, bf16[8,512,256]{2,1,0:T(8,128)(2,1)S(1)}, u32[]{:S(2)}, u32[]{:S(2)}) collective-permute-start(bf16[8,512,256]{2,1,0:T(8,128)(2,1)S(1)} %select_convert_fusion), channel_id=1, source_target_pairs={{0,4},{4,0},{2,6},{6,2},{8,12},{12,8},{10,14},{14,10},{16,20},{20,... | collective-permute-start | bytes 6291464 | tf_op jit(solution)/shard_map/ppermute | solution.py:25
  141.9 7.5 %collective-permute-start.14 = (bf16[15,512]{1,0:T(8,128)(2,1)S(1)}, bf16[15,512]{1,0:T(8,128)(2,1)S(1)}, u32[]{:S(2)}, u32[]{:S(2)}) collective-permute-start(bf16[15,512]{1,0:T(8,128)(2,1)S(1)} %slice.241), channel_id=1, source_target_pairs={{0,2},{2,4},{4,6},{6,8},{8,10},{10,12},{12,14},{14,16},{16,18},{18... | collective-permute-start | bytes 46088 | tf_op jit(solution)/shard_map/ppermute | solution.py:15
  145.2 33.1 %collective-permute-start.12 = (bf16[8,512]{1,0:T(8,128)(2,1)S(1)}, bf16[8,512]{1,0:T(8,128)(2,1)S(1)}, u32[]{:S(2)}, u32[]{:S(2)}) collective-permute-start(bf16[8,512]{1,0:T(8,128)(2,1)S(1)} %select_convert_fusion.2), channel_id=1, source_target_pairs={{0,4},{4,0},{2,6},{6,2},{8,12},{12,8},{10,14},{14,10},{16,20},{20,... | collective-permute-start | bytes 24584 | tf_op jit(solution)/shard_map/ppermute | solution.py:25
  146.6 31.9 %collective-permute-start.8 = (bf16[8,512]{1,0:T(8,128)(2,1)S(1)}, bf16[8,512]{1,0:T(8,128)(2,1)S(1)}, u32[]{:S(2)}, u32[]{:S(2)}) collective-permute-start(bf16[8,512]{1,0:T(8,128)(2,1)S(1)} %select_convert_fusion.3), channel_id=1, source_target_pairs={{0,4},{4,0},{2,6},{6,2},{8,12},{12,8},{10,14},{14,10},{16,20},{20,... | collective-permute-start | bytes 24584 | tf_op jit(solution)/shard_map/ppermute | solution.py:25
  178.5 7.7 %copy-start.13 = (bf16[4,128,128]{2,1,0:T(8,128)(2,1)S(1)}, bf16[4,128,128]{2,1,0:T(8,128)(2,1)}, u32[]{:S(2)}) copy-start(bf16[4,128,128]{2,1,0:T(8,128)(2,1)} %param.23) | copy-start | bytes 393220
  183.4 13.8 %collective-permute-start.11 = (bf16[8,256,256]{2,1,0:T(8,128)(2,1)S(1)}, bf16[8,256,256]{2,1,0:T(8,128)(2,1)S(1)}, u32[]{:S(2)}, u32[]{:S(2)}) collective-permute-start(bf16[8,256,256]{2,1,0:T(8,128)(2,1)S(1)} %select_convert_fusion.1), channel_id=1, source_target_pairs={{0,2},{2,0},{4,6},{6,4},{8,10},{10,8},{12,14},{14,12},{16,18},{18,... | collective-permute-start | bytes 3145736 | tf_op jit(solution)/shard_map/ppermute | solution.py:25
  184.7 12.5 %collective-permute-start.13 = (bf16[8,256]{1,0:T(8,128)(2,1)S(1)}, bf16[8,256]{1,0:T(8,128)(2,1)S(1)}, u32[]{:S(2)}, u32[]{:S(2)}) collective-permute-start(bf16[8,256]{1,0:T(8,128)(2,1)S(1)} %select_convert_fusion.4), channel_id=1, source_target_pairs={{0,2},{2,0},{4,6},{6,4},{8,10},{10,8},{12,14},{14,12},{16,18},{18,... | collective-permute-start | bytes 12296 | tf_op jit(solution)/shard_map/ppermute | solution.py:25
  184.9 12.3 %collective-permute-start.10 = (bf16[8,256]{1,0:T(8,128)(2,1)S(1)}, bf16[8,256]{1,0:T(8,128)(2,1)S(1)}, u32[]{:S(2)}, u32[]{:S(2)}) collective-permute-start(bf16[8,256]{1,0:T(8,128)(2,1)S(1)} %select_convert_fusion.5), channel_id=1, source_target_pairs={{0,2},{2,0},{4,6},{6,4},{8,10},{10,8},{12,14},{14,12},{16,18},{18,... | collective-permute-start | bytes 12296 | tf_op jit(solution)/shard_map/ppermute | solution.py:25
  198.2 0.7 copy-start.8
Sparse Core Ops, SparseCore 0:
  8.9 10.8 all-gather.1
  204.7 57.8 reduce-scatter.1
where the time goes:
time: 271 us; the launch traced here: 269 us
  waiting for transfers between devices  154 us (57%)
  other arithmetic  42.3 us (16%)
  matrix products  33 us (12%)
  starting transfers between devices  14.5 us (5%)
  between operations  13.7 us (5%)
  local copies, waits for them, and re-layouts  11.7 us (4%)
    reduce_scatter x1, waiting for transfers between devices, per_device(): lax.psum_scatter((partial_value + jnp.dot(pool_out, pool_out_weight, pref...  58 us
    ppermute x8, waiting for transfers between devices, from_partner(): return lax.ppermute(block, axis, route)  55.6 us
    ppermute x6, waiting for transfers between devices, shifted(): lax.ppermute(array, axis, [(i, (i + by) % size) for i in range(size)])  24.5 us
    add x3, other arithmetic, block_work(): weighted * shrink[:, :, None] + update.reshape(unit_count, query_count, -1)  19.3 us
    all_gather x1, waiting for transfers between devices, per_device(): project_incoming = lax.all_gather(normed, 'tp', axis=0, tiled=True)  12.4 us
    dot_general x4, matrix products, per_device(): jnp.dot(project_incoming, weight_part, preferred_element_type=jnp.float32)  9.77 us
    dot_general x3, matrix products, block_work(): jnp.einsum('qud,kud->uqk', queries, key_rows, preferred_element_type=jnp....  9.37 us
    dot_general x3, matrix products, block_work(): jnp.einsum('hmqk,khe->hmqe', map_weights, value_rows, preferred_element_t...  7.4 us
  transfers between devices with their start and end apart: 17, of which 11 were waited for; matrix products, arithmetic and copies ran while one was open for 24% of the time, Pallas kernels for 0%

commit v1 on v0

v1 whole, which is shorter than its diff:
```python
import functools
import math

import jax
import jax.numpy as jnp
from jax import lax
from jax.experimental import pallas as pl
from jax.experimental.pallas import tpu as pltpu
from jax.sharding import PartitionSpec as P

norm_epsilon = 1e-06
halo = 16
log2e = math.log2(math.e)

VMEM = pltpu.VMEM
SMEM = pltpu.SMEM


def dot(a, b):
    return jnp.dot(a, b, preferred_element_type=jnp.float32)


def dot_t(a, b):
    return lax.dot_general(a, b, (((1,), (1,)), ((), ())), preferred_element_type=jnp.float32)


def cost(flops, nbytes, exps=0):
    return pl.CostEstimate(flops=int(flops), bytes_accessed=int(nbytes), transcendentals=int(exps))


def params(*semantics, mib=48):
    return pltpu.CompilerParams(dimension_semantics=semantics, vmem_limit_bytes=mib << 20)


def project_body(n_w, scalars, mine, other, *rest):
    weights, out, rows, acc = rest[:n_w], rest[n_w], rest[n_w + 1], rest[n_w + 2]
    step = pl.program_id(0)
    half = mine.shape[0]
    first = pl.multiple_of(scalars[1] * half, half)
    second = pl.multiple_of((1 - scalars[1]) * half, half)
    rows[pl.ds(first, half), :] = mine[...]
    rows[pl.ds(second, half), :] = other[...]
    x = rows[...]
    width = weights[0].shape[1]
    for n in range(n_w):
        part = dot(x, weights[n][...])
        cols = slice(n * width, (n + 1) * width)

        @pl.when(step == 0)
        def _():
            acc[:, cols] = part

        @pl.when(step > 0)
        def _():
            acc[:, cols] += part

    @pl.when(step == pl.num_programs(0) - 1)
    def _():
        out[...] = acc[...].astype(out.dtype)


def project(head, which, mine, other, weights, width):
    half, depth = mine.shape
    tiles = 4
    tile = depth // tiles
    n_w = len(weights)
    scalars = jnp.stack([head, which]).astype(jnp.int32)
    grid_spec = pltpu.PrefetchScalarGridSpec(
        num_scalar_prefetch=1,
        grid=(tiles,),
        in_specs=[pl.BlockSpec((half, tile), lambda i, sc: (0, i))] * 2
        + [pl.BlockSpec((tile, width), lambda i, sc: (i, sc[0]))] * n_w,
        out_specs=pl.BlockSpec((2 * half, n_w * width), lambda i, sc: (0, 0)),
        scratch_shapes=[
            pltpu.VMEM((2 * half, tile), jnp.bfloat16),
            pltpu.VMEM((2 * half, n_w * width), jnp.float32),
        ],
    )
    return pl.pallas_call(
        functools.partial(project_body, n_w),
        grid_spec=grid_spec,
        out_shape=jax.ShapeDtypeStruct((2 * half, n_w * width), jnp.bfloat16),
        compiler_params=params("arbitrary", mib=24),
        cost_estimate=cost(4 * half * depth * n_w * width, 2 * depth * n_w * width),
        name="project",
    )(scalars, mine, other, *weights)


def pool_body(groups, scalars, mine, other, rim, w_in, w_mix, w_out, out, rows, mixed):
    half = mine.shape[0]
    count = 2 * half
    which, tp_index, sp_index = scalars[0], scalars[1], scalars[2]
    first = pl.multiple_of(halo + which * half, halo)
    second = pl.multiple_of(halo + (1 - which) * half, halo)
    rows[0:halo, :] = rim[...]
    rows[pl.ds(first, half), :] = mine[...]
    rows[pl.ds(second, half), :] = other[...]
    pooled = dot(rows[...], w_in[...]).astype(jnp.bfloat16).astype(jnp.float32)
    index = lax.broadcasted_iota(jnp.int32, pooled.shape, 0)
    pooled = jnp.where((index < halo) & (sp_index == 0), 0.0, pooled)
    sums = []
    total = pooled
    for bit in range(4):
        total = total + pltpu.roll(total, 1 << bit, 0)
        sums.append(total)
    width = w_mix.shape[1]
    position = sp_index * count + lax.broadcasted_iota(jnp.int32, (count, width), 0)
    for g in range(groups):
        kind = lax.rem(tp_index * groups + g, 4)
        cols = slice(g * width, (g + 1) * width)
        picked = sums[0][halo:, cols]
        for bit in range(1, 4):
            picked = jnp.where(kind == bit, sums[bit][halo:, cols], picked)
        window = jnp.left_shift(jnp.int32(2), kind)
        counts = jnp.minimum(position + 1, window).astype(jnp.float32)
        spread = (picked / counts - pooled[halo:, cols]).astype(jnp.bfloat16)
        mixed[:, cols] = dot(spread, w_mix[g]).astype(jnp.bfloat16)
    out[...] = dot(mixed[...], w_out[...])


def pool(which, tp_index, sp_index, mine, other, rim, w_in, w_mix, w_out):
    half, depth = mine.shape
    cols = w_in.shape[1]
    scalars = jnp.stack([which, tp_index, sp_index]).astype(jnp.int32)
    return pl.pallas_call(
        functools.partial(pool_body, w_mix.shape[0]),
        in_specs=[pl.BlockSpec(memory_space=SMEM)] + [pl.BlockSpec(memory_space=VMEM)] * 6,
        out_specs=pl.BlockSpec(memory_space=VMEM),
        out_shape=jax.ShapeDtypeStruct((2 * half, w_out.shape[1]), jnp.float32),
        scratch_shapes=[
            pltpu.VMEM((2 * half + halo, depth), jnp.bfloat16),
            pltpu.VMEM((2 * half, cols), jnp.bfloat16),
        ],
        compiler_params=params(mib=32),
        cost_estimate=cost(8 * half * depth * cols, 8 * depth * cols),
        name="pool",
    )(scalars, mine, other, rim, w_in, w_mix, w_out)


def softmax_parts(scores, old_peak, scale):
    peak = old_peak
    for s in scores:
        top = jnp.max(s, axis=1, keepdims=True)
        peak = top if peak is None else jnp.maximum(peak, top)
    weights, total = [], None
    for s in scores:
        raised = jnp.exp2((s - peak) * scale)
        part = jnp.sum(raised, axis=1, keepdims=True)
        total = part if total is None else total + part
        weights.append(raised.astype(jnp.bfloat16))
    return peak, total, weights


def own_body(heads, rows, scale, scalars, *refs):
    own, partner = refs[:heads], refs[heads : 2 * heads]
    q_out, stat_out, acc_out, keys, values, sems = refs[2 * heads :]
    slot, parity = scalars[0], scalars[1]
    width = keys.shape[1]
    dim = width // 2
    copies = []
    for k in range(heads):
        place = jnp.bitwise_xor(k, slot)
        q_at = pl.multiple_of(place * rows, rows)
        own_at = pl.multiple_of((2 * place + parity) * rows, rows)
        partner_at = pl.multiple_of((2 * place + 1 - parity) * rows, rows)
        for source, target in (
            (own[k].at[:, 0:width], q_out.at[pl.ds(q_at, rows), :]),
            (own[k].at[:, width : 2 * width], keys.at[pl.ds(own_at, rows), :]),
            (own[k].at[:, 2 * width : 3 * width], values.at[pl.ds(own_at, rows), :]),
            (partner[k].at[:, width : 2 * width], keys.at[pl.ds(partner_at, rows), :]),
            (partner[k].at[:, 2 * width : 3 * width], values.at[pl.ds(partner_at, rows), :]),
        ):
            copies.append(pltpu.make_async_copy(source, target, sems.at[len(copies)]))
    for copy in copies:
        copy.start()
    for copy in copies:
        copy.wait()
    lane = lax.broadcasted_iota(jnp.int32, (rows, 128), 1)
    row = lax.broadcasted_iota(jnp.int32, (rows, 2 * rows), 0)
    col = lax.broadcasted_iota(jnp.int32, (rows, 2 * rows), 1)
    allowed = col <= row + parity * rows
    for i in range(heads):
        q_rows = slice(i * rows, (i + 1) * rows)
        for c in range(2):
            cols = slice(c * dim, (c + 1) * dim)
            q = q_out[q_rows, cols]
            before = 2 * i * rows
            scores = []
            if before:
                scores.append(dot_t(q, keys[0:before, cols]))
            edge = dot_t(q, keys[before : before + 2 * rows, cols])
            scores.append(jnp.where(allowed, edge, -jnp.inf))
            peak, total, weights = softmax_parts(scores, None, scale)
            acc = dot(weights[-1], values[before : before + 2 * rows, :])
            if before:
                acc = acc + dot(weights[0], values[0:before, :])
            acc_out[c, q_rows, :] = acc
            stat_out[c, q_rows, :] = jnp.where(lane < 64, peak, total)


def attend_own(slot, parity, own, partner, scale):
    heads = len(own)
    rows, width = own[0].shape[0], own[0].shape[1] // 3
    count = heads * rows
    scalars = jnp.stack([slot, parity]).astype(jnp.int32)
    pairs = 2 * count * 2 * count
    return pl.pallas_call(
        functools.partial(own_body, heads, rows, scale * log2e),
        in_specs=[pl.BlockSpec(memory_space=SMEM)]
        + [pl.BlockSpec(memory_space=pl.ANY)] * (2 * heads),
        out_specs=[pl.BlockSpec(memory_space=VMEM)] * 3,
        out_shape=[
            jax.ShapeDtypeStruct((count, width), jnp.bfloat16),
            jax.ShapeDtypeStruct((2, count, 128), jnp.float32),
            jax.ShapeDtypeStruct((2, count, width), jnp.float32),
        ],
        scratch_shapes=[
            pltpu.VMEM((2 * count, width), jnp.bfloat16),
            pltpu.VMEM((2 * count, width), jnp.bfloat16),
            pltpu.SemaphoreType.DMA((5 * heads,)),
        ],
        compiler_params=params(mib=40),
        cost_estimate=cost(pairs * width * 2, 4 * count * width * 4, pairs),
        name="attend_own",
    )(scalars, *own, *partner)


def cross_body(blocks, heads, rows, scale, final, scalars, balance, gain, q_in, stat_in, acc_in, *refs):
    pieces, outs = refs[:blocks], refs[blocks:]
    width = q_in.shape[1]
    dim = width // 2
    active, slot, head = scalars[0], scalars[1], scalars[2]
    if final:
        done, stat_out, acc_out = outs[heads], outs[heads + 1], outs[heads + 2]
    else:
        stat_out, acc_out = outs
    lane = lax.broadcasted_iota(jnp.int32, (rows, 128), 1)

    @pl.when(active == 1)
    def _():
        for i in range(heads):
            q_rows = slice(i * rows, (i + 1) * rows)
            for c in range(2):
                cols = slice(c * dim, (c + 1) * dim)
                q = q_in[q_rows, cols]
                old_peak = stat_in[c, q_rows, 0:1]
                old_total = stat_in[c, q_rows, 64:65]
                scores = [dot_t(q, piece[:, cols]) for piece in pieces]
                peak, total, weights = softmax_parts(scores, old_peak, scale)
                shrink = jnp.exp2((old_peak - peak) * scale)
                acc = acc_in[c, q_rows, :] * shrink
                for weight, piece in zip(weights, pieces):
                    acc = acc + dot(weight, piece[:, width : 2 * width])
                acc_out[c, q_rows, :] = acc
                stat_out[c, q_rows, :] = jnp.where(lane < 64, peak, old_total * shrink + total)

    @pl.when(active == 0)
    def _():
        stat_out[...] = stat_in[...]
        acc_out[...] = acc_in[...]

    if final:
        factor = balance[head]
        for i in range(heads):
            q_rows = slice(i * rows, (i + 1) * rows)
            maps = [
                (acc_out[c, q_rows, :] / stat_out[c, q_rows, 64:65])
                .astype(jnp.bfloat16)
                .astype(jnp.float32)
                for c in range(2)
            ]
            contrast = maps[0] - factor * maps[1]
            square = jnp.mean(contrast * contrast, axis=1, keepdims=True)
            contrast = contrast * lax.rsqrt(square + norm_epsilon) * gain[...]
            done[q_rows, :] = contrast.astype(jnp.bfloat16)
        for k in range(heads):
            place = jnp.bitwise_xor(k, slot)
            outs[k][...] = done[pl.ds(pl.multiple_of(place * rows, rows), rows), :]


def attend_cross(active, slot, head, balance, gain, state, pieces, heads, scale, final):
    q, stat, acc = state
    count, width = q.shape
    rows = count // heads
    scalars = jnp.stack([active, slot, head]).astype(jnp.int32)
    pairs = 2 * count * rows * len(pieces)
    state_shapes = [
        jax.ShapeDtypeStruct(stat.shape, jnp.float32),
        jax.ShapeDtypeStruct(acc.shape, jnp.float32),
    ]
    if final:
        out_shape = [jax.ShapeDtypeStruct((rows, width), jnp.bfloat16)] * heads
        scratch = [
            pltpu.VMEM((count, width), jnp.bfloat16),
            pltpu.VMEM(stat.shape, jnp.float32),
            pltpu.VMEM(acc.shape, jnp.float32),
        ]
    else:
        out_shape, scratch = state_shapes, []
    return pl.pallas_call(
        functools.partial(cross_body, len(pieces), heads, rows, scale * log2e, final),
        in_specs=[pl.BlockSpec(memory_space=SMEM)] * 2
        + [pl.BlockSpec(memory_space=VMEM)] * (4 + len(pieces)),
        out_specs=[pl.BlockSpec(memory_space=VMEM)] * len(out_shape),
        out_shape=out_shape,
        scratch_shapes=scratch,
        compiler_params=params(mib=48),
        cost_estimate=cost(pairs * width * 3, 8 * count * width, pairs),
        name="attend_cross",
    )(scalars, balance, gain, q, stat, acc, *pieces)


def output_body(heads, scalars, *refs):
    blocks, weight, pooled, out = refs[:heads], refs[heads], refs[heads + 1], refs[heads + 2]
    half, tile = out.shape
    width = blocks[0].shape[1]
    start = pl.multiple_of(scalars[1] * half, half)
    total = pooled[pl.ds(start, half), :]
    for k in range(heads):
        place = jnp.bitwise_xor(k, scalars[0])
        part = weight[pl.ds(pl.multiple_of(place * width, width), width), :]
        total = total + dot(blocks[k][pl.ds(start, half), :], part)
    out[...] = total.astype(out.dtype)


def output(slot, part, blocks, weight, pooled, dtype):
    heads = len(blocks)
    rows, width = blocks[0].shape
    depth, model = weight.shape
    half = rows // 2
    tiles = 4
    tile = model // tiles
    scalars = jnp.stack([slot, part]).astype(jnp.int32)
    grid_spec = pltpu.PrefetchScalarGridSpec(
        num_scalar_prefetch=1,
        grid=(tiles,),
        in_specs=[pl.BlockSpec((rows, width), lambda i, sc: (0, 0))] * heads
        + [
            pl.BlockSpec((depth, tile), lambda i, sc: (0, i)),
            pl.BlockSpec((rows, tile), lambda i, sc: (0, i)),
        ],
        out_specs=pl.BlockSpec((half, tile), lambda i, sc: (0, i)),
    )
    return pl.pallas_call(
        functools.partial(output_body, heads),
        grid_spec=grid_spec,
        out_shape=jax.ShapeDtypeStruct((half, model), dtype),
        compiler_params=params("arbitrary", mib=24),
        cost_estimate=cost(2 * half * depth * model, 2 * depth * model),
        name="output",
    )(scalars, *blocks, weight, pooled)


def per_device(
    normed,
    query_weight,
    key_weight,
    value_weight,
    pool_in_weight,
    pool_weight,
    map_balance,
    head_gain,
    contrast_out_weight,
    pool_out_weight,
):
    sp_count, tp_count = lax.axis_size("sp"), lax.axis_size("tp")
    s, t = lax.axis_index("sp"), lax.axis_index("tp")
    width = head_gain.shape[0]
    dim = width // 2
    heads = query_weight.shape[1] // width
    members = 2 * heads
    groups = sp_count // members
    scale = dim ** (-0.5)
    both = ("sp", "tp")
    swap = [(i, i ^ 1) for i in range(tp_count)]

    def exchange_route(k, first_group, back):
        route = []
        for source in range(first_group * members, sp_count):
            m = source % members
            base = source - m
            for core in range(tp_count):
                local = k ^ (m >> 1)
                target = base + (core & 1) * heads + local
                target_core = (core & ~1) | (m & 1)
                pair = (source * tp_count + core, target * tp_count + target_core)
                route.append(pair[::-1] if back else pair)
        return route

    def spread_out(parts, first_group=0, back=False):
        return [
            lax.ppermute(part, both, exchange_route(k, first_group, back))
            for k, part in enumerate(parts)
        ]

    def across(block):
        return lax.ppermute(block, "tp", swap)

    def whole_rows(block):
        if tp_count == 2:
            return block, across(block), t
        full = lax.all_gather(block, "tp", axis=0, tiled=True)
        half = full.shape[0] // 2
        return full[:half], full[half:], jnp.int32(0)

    member = s % members
    group = s // members
    send_slot = member >> 1
    own_slot = member % heads
    parity = t & 1

    mine, other, which = whole_rows(normed)
    far = [
        lax.ppermute(
            normed, "sp", [(i, i + members) for i in range(sp_count - members)]
        )
    ]
    sent = [
        project(
            jnp.bitwise_xor(k, send_slot),
            which,
            mine,
            other,
            (query_weight, key_weight, value_weight),
            width,
        )
        for k in range(heads)
    ]
    own = spread_out(sent)
    partner = [across(block) for block in own]

    last = jnp.where(which == 0, other[-halo:], mine[-halo:])
    rim = lax.ppermute(last, "sp", [(i, (i + 1) % sp_count) for i in range(sp_count)])
    pooled = pool(
        which, t, s, mine, other, rim, pool_in_weight, pool_weight, pool_out_weight
    )

    q, stat, acc = attend_own(own_slot, parity, own, partner, scale)

    head = (t - parity) * heads + member
    gain = head_gain.reshape(1, width)

    def cross(rows_here, step, stat, acc, first_group, final):
        mine, other, which = whole_rows(rows_here)
        sent = [
            project(
                jnp.bitwise_xor(k, send_slot), which, mine, other, (key_weight, value_weight), width
            )
            for k in range(heads)
        ]
        got = spread_out(sent, first_group)
        pieces = got + [across(block) for block in got]
        active = (group >= step).astype(jnp.int32)
        return attend_cross(
            active, own_slot, head, map_balance, gain, (q, stat, acc), pieces, heads, scale, final
        )

    if groups == 2:
        done = cross(far[0], 1, stat, acc, 1, True)
    else:
        ring = [(i, (i + members) % sp_count) for i in range(sp_count)]

        def body(step, carry):
            rows_here, stat, acc = carry
            stat, acc = cross(rows_here, step, stat, acc, 0, False)
            return lax.ppermute(rows_here, "sp", ring), stat, acc

        rows_here, stat, acc = lax.fori_loop(
            1, groups - 1, body, (lax.ppermute(normed, "sp", ring), stat, acc)
        )
        done = cross(rows_here, groups - 1, stat, acc, 0, True)

    returned = spread_out(done, back=True)
    if tp_count == 2:
        given = output(send_slot, 1 - t, returned, contrast_out_weight, pooled, jnp.bfloat16)
        taken = across(given)
        kept = output(send_slot, t, returned, contrast_out_weight, pooled, jnp.bfloat16)
        return (kept.astype(jnp.float32) + taken.astype(jnp.float32)).astype(jnp.bfloat16)
    halves = [
        output(send_slot, jnp.int32(p), returned, contrast_out_weight, pooled, jnp.bfloat16)
        for p in range(2)
    ]
    return lax.psum_scatter(
        jnp.concatenate(halves, axis=0), "tp", scatter_dimension=0, tiled=True
    )


def solution(mesh):
    return jax.shard_map(
        per_device,
        mesh=mesh,
        in_specs=(
            P(("sp", "tp"), None),
            P(None, "tp"),
            P(None, "tp"),
            P(None, "tp"),
            P(None, "tp"),
            P("tp", None, None),
            P(),
            P(),
            P("tp", None),
            P("tp", None),
        ),
        out_specs=P(("sp", "tp"), None),
        check_vma=False,
    )
```

time: 271 us -> 139 us (0.51)
  waiting for transfers between devices: 154 us -> 9.97 us
  Pallas kernels: 0 us -> 58.3 us
  other arithmetic: 42.3 us -> 1.54 us
  matrix products: 33 us -> 0 us
  starting transfers between devices: 14.5 us -> 41.9 us
  local copies, waits for them, and re-layouts: 11.7 us -> 26.5 us
  between operations: 13.7 us -> 0.48 us
    ppermute x15 -> x25, waiting for transfers between devices: 82.7 us -> 9.97 us  [the longest x12 9.65 us: spread_out(): lax.ppermute(part, both, exchange_route(k, first_group, back))]
    pallas_call x0 -> x13, Pallas kernels: none -> 58.3 us  [the longest x8 33.3 us: project(): pl.pallas_call(functools.partial(project_body, n_w), grid_spec=grid_spec,...]
    reduce_scatter x1 -> x0, waiting for transfers between devices: 58 us -> none  [per_device(): lax.psum_scatter((partial_value + jnp.dot(pool_out, pool_out_weight, pref...]
    dot_general x13 -> x0, matrix products: 33 us -> none  [the longest x4 9.77 us: per_device(): jnp.dot(project_incoming, weight_part, preferred_element_type=jnp.float32)]
    ppermute x15 -> x25, starting transfers between devices: 14.4 us -> 41.9 us  [the longest x12 38.5 us: spread_out(): lax.ppermute(part, both, exchange_route(k, first_group, back))]
    add x14 -> x0, other arithmetic: 24.1 us -> none  [the longest x3 19.3 us: block_work(): weighted * shrink[:, :, None] + update.reshape(unit_count, query_count, -1)]
    unnamed x29 -> x48, local copies, waits for them, and re-layouts: 3.2 us -> 26.5 us
    all_gather x1 -> x0, waiting for transfers between devices: 12.4 us -> none  [per_device(): project_incoming = lax.all_gather(normed, 'tp', axis=0, tiled=True)]
  transfers between devices with their start and end apart: 17 -> 25, of which waited for: 11 -> 4; matrix products, arithmetic and copies ran while one was open for 24% -> 0% of each run, Pallas kernels for 0% -> 40%
where the time goes in v1:
time: 139 us
  Pallas kernels  58.3 us (42%)
  starting transfers between devices  41.9 us (30%)
  local copies, waits for them, and re-layouts  26.5 us (19%)
  waiting for transfers between devices  9.97 us (7%)
  other arithmetic  1.54 us (1%)
    ppermute x12, starting transfers between devices, spread_out(): lax.ppermute(part, both, exchange_route(k, first_group, back))  38.5 us
    pallas_call x8, Pallas kernels, project(): pl.pallas_call(functools.partial(project_body, n_w), grid_spec=grid_spec,...  33.3 us
    unnamed x48, local copies, waits for them, and re-layouts  26.5 us
    pallas_call x1, Pallas kernels, attend_cross(): pl.pallas_call(functools.partial(cross_body, len(pieces), heads, rows, sc...  10.9 us
    ppermute x12, waiting for transfers between devices, spread_out(): lax.ppermute(part, both, exchange_route(k, first_group, back))  9.65 us
    pallas_call x1, Pallas kernels, attend_own(): pl.pallas_call(functools.partial(own_body, heads, rows, scale * log2e), i...  7.03 us
    pallas_call x2, Pallas kernels, output(): pl.pallas_call(functools.partial(output_body, heads), grid_spec=grid_spec...  4.67 us
  transfers between devices with their start and end apart: 25, of which 4 were waited for; matrix products, arithmetic and copies ran while one was open for 0% of the time, Pallas kernels for 40%

profile of v1, /device:TPU:17, one launch (start us, length us, event | category | flops | bytes accessed | tf_op | source)
XLA Modules:
  0.0 138.7 jit_solution(7107626915753538778)
XLA Ops:
  0.0 0.7 collective-permute-start
  0.7 1.3 collective-permute-start.9
  2.0 0.1 pad_add_fusion.7.scalars
  2.1 0.1 pad_add_fusion.2.scalars
  2.1 0.3 collective-permute-done.other
  2.4 2.2 %copy-done = bf16[2048,1024]{1,0:T(8,128)(2,1)S(1)} copy-done((bf16[2048,1024]{1,0:T(8,128)(2,1)S(1)}, bf16[2048,1024]{1,0:T(8,128)(2,1)}, u32[]{:S(2)}) %copy-start) | copy-done | bytes 4194328
  4.6 2.2 %copy-done.6 = bf16[2048,1024]{1,0:T(8,128)(2,1)S(1)} copy-done((bf16[2048,1024]{1,0:T(8,128)(2,1)S(1)}, bf16[2048,1024]{1,0:T(8,128)(2,1)}, u32[]{:S(2)}) %copy-start.6) | copy-done | bytes 4194328
  6.8 2.2 %copy-done.12 = bf16[2048,1024]{1,0:T(8,128)(2,1)S(1)} copy-done((bf16[2048,1024]{1,0:T(8,128)(2,1)S(1)}, bf16[2048,1024]{1,0:T(8,128)(2,1)}, u32[]{:S(2)}) %copy-start.12) | copy-done | bytes 4194328
  9.0 1.0 copy-done.16
  10.0 4.7 %project.8 = bf16[256,768]{1,0:T(8,128)(2,1)S(1)} custom-call(s32[2]{0:T(128)S(1)} %pad_add_fusion.7.scalars, bf16[128,2048]{1,0:T(8,128)(2,1)S(1)} %copy-done.16, bf16[128,2048]{1,0:T(8,128)(2,1)S(1)} %collective-permute-done.other, bf16[2048,1024]{1,0:T(8,128)(2,1)S(1)} %copy-done.12, bf16[2048,1024]{1,0:T(8,128)(2,1)S(1)} %copy-done, ...), custom_call_target="tpu_custom_call" | custom-call | flops 805306368 | bytes 3145728 | tf_op jit(solution)/shard_map/project/pallas_call | solution.py:79
  14.7 3.5 %collective-permute-start.1 = (bf16[256,768]{1,0:T(8,128)(2,1)S(1)}, bf16[256,768]{1,0:T(8,128)(2,1)}, u32[]{:S(2)}, u32[]{:S(2)}) collective-permute-start(bf16[256,768]{1,0:T(8,128)(2,1)S(1)} %project.8), channel_id=1, source_target_pairs={{0,0},{1,8},{2,1},{3,9},{4,2},{5,10},{6,3},{7,11},{8,4},{9,12},{10... | collective-permute-start | bytes 1179656 | tf_op jit(solution)/shard_map/ppermute | solution.py:392
  18.2 4.7 %project.9 = bf16[256,768]{1,0:T(8,128)(2,1)S(1)} custom-call(s32[2]{0:T(128)S(1)} %pad_add_fusion.2.scalars, bf16[128,2048]{1,0:T(8,128)(2,1)S(1)} %copy-done.17, bf16[128,2048]{1,0:T(8,128)(2,1)S(1)} %collective-permute-done.other, bf16[2048,1024]{1,0:T(8,128)(2,1)S(1)} %copy-done.12, bf16[2048,1024]{1,0:T(8,128)(2,1)S(1)} %copy-done.1, ...), custom_call_target="tpu_custom_call" | custom-call | flops 805306368 | bytes 3145728 | tf_op jit(solution)/shard_map/project/pallas_call | solution.py:79
  22.9 2.1 %collective-permute-start.2 = (bf16[256,768]{1,0:T(8,128)(2,1)S(1)}, bf16[256,768]{1,0:T(8,128)(2,1)}, u32[]{:S(2)}, u32[]{:S(2)}) collective-permute-start(bf16[256,768]{1,0:T(8,128)(2,1)S(1)} %project.9), channel_id=1, source_target_pairs={{0,2},{1,10},{2,3},{3,11},{4,0},{5,8},{6,1},{7,9},{8,6},{9,14},{10... | collective-permute-start | bytes 1179656 | tf_op jit(solution)/shard_map/ppermute | solution.py:392
  25.0 0.1 pad_add_fusion.3.scalars
  25.1 2.2 %copy-done.2 = bf16[2048,1024]{1,0:T(8,128)(2,1)S(1)} copy-done((bf16[2048,1024]{1,0:T(8,128)(2,1)S(1)}, bf16[2048,1024]{1,0:T(8,128)(2,1)}, u32[]{:S(2)}) %copy-start.2) | copy-done | bytes 4194328
  27.3 2.2 %copy-done.8 = bf16[2048,1024]{1,0:T(8,128)(2,1)S(1)} copy-done((bf16[2048,1024]{1,0:T(8,128)(2,1)S(1)}, bf16[2048,1024]{1,0:T(8,128)(2,1)}, u32[]{:S(2)}) %copy-start.8) | copy-done | bytes 4194328
  29.5 2.2 %copy-done.13 = bf16[2048,1024]{1,0:T(8,128)(2,1)S(1)} copy-done((bf16[2048,1024]{1,0:T(8,128)(2,1)S(1)}, bf16[2048,1024]{1,0:T(8,128)(2,1)}, u32[]{:S(2)}) %copy-start.13) | copy-done | bytes 4194328
  31.6 5.4 %project.10 = bf16[256,768]{1,0:T(8,128)(2,1)} custom-call(s32[2]{0:T(128)S(1)} %pad_add_fusion.3.scalars, bf16[128,2048]{1,0:T(8,128)(2,1)S(1)} %copy-done.17, bf16[128,2048]{1,0:T(8,128)(2,1)S(1)} %collective-permute-done.other, bf16[2048,1024]{1,0:T(8,128)(2,1)S(1)} %copy-done.13, bf16[2048,1024]{1,0:T(8,128)(2,1)S(1)} %copy-done.2, ...), custom_call_target="tpu_custom_call" | custom-call | flops 805306368 | bytes 3145728 | tf_op jit(solution)/shard_map/project/pallas_call | solution.py:79
  37.0 6.4 %collective-permute-start.3 = (bf16[256,768]{1,0:T(8,128)(2,1)}, bf16[256,768]{1,0:T(8,128)(2,1)}, u32[]{:S(2)}, u32[]{:S(2)}) collective-permute-start(bf16[256,768]{1,0:T(8,128)(2,1)} %project.10), channel_id=1, source_target_pairs={{0,4},{1,12},{2,5},{3,13},{4,6},{5,14},{6,7},{7,15},{8,0},{9,8},{1... | collective-permute-start | bytes 1179656 | tf_op jit(solution)/shard_map/ppermute | solution.py:392
  43.4 0.1 pad_add_fusion.4.scalars
  43.5 2.2 %copy-done.3 = bf16[2048,1024]{1,0:T(8,128)(2,1)S(1)} copy-done((bf16[2048,1024]{1,0:T(8,128)(2,1)S(1)}, bf16[2048,1024]{1,0:T(8,128)(2,1)}, u32[]{:S(2)}) %copy-start.3) | copy-done | bytes 4194328
  45.7 2.2 %copy-done.9 = bf16[2048,1024]{1,0:T(8,128)(2,1)S(1)} copy-done((bf16[2048,1024]{1,0:T(8,128)(2,1)S(1)}, bf16[2048,1024]{1,0:T(8,128)(2,1)}, u32[]{:S(2)}) %copy-start.9) | copy-done | bytes 4194328
  47.9 2.2 %copy-done.14 = bf16[2048,1024]{1,0:T(8,128)(2,1)S(1)} copy-done((bf16[2048,1024]{1,0:T(8,128)(2,1)S(1)}, bf16[2048,1024]{1,0:T(8,128)(2,1)}, u32[]{:S(2)}) %copy-start.14) | copy-done | bytes 4194328
  50.1 4.7 %project.11 = bf16[256,768]{1,0:T(8,128)(2,1)S(1)} custom-call(s32[2]{0:T(128)S(1)} %pad_add_fusion.4.scalars, bf16[128,2048]{1,0:T(8,128)(2,1)S(1)} %copy-done.17, bf16[128,2048]{1,0:T(8,128)(2,1)S(1)} %collective-permute-done.other, bf16[2048,1024]{1,0:T(8,128)(2,1)S(1)} %copy-done.14, bf16[2048,1024]{1,0:T(8,128)(2,1)S(1)} %copy-done.3, ...), custom_call_target="tpu_custom_call" | custom-call | flops 805306368 | bytes 3145728 | tf_op jit(solution)/shard_map/project/pallas_call | solution.py:79
  54.7 2.9 %collective-permute-start.4 = (bf16[256,768]{1,0:T(8,128)(2,1)S(1)}, bf16[256,768]{1,0:T(8,128)(2,1)}, u32[]{:S(2)}, u32[]{:S(2)}) collective-permute-start(bf16[256,768]{1,0:T(8,128)(2,1)S(1)} %project.11), channel_id=1, source_target_pairs={{0,6},{1,14},{2,7},{3,15},{4,4},{5,12},{6,5},{7,13},{8,2},{9,10},{... | collective-permute-start | bytes 1179656 | tf_op jit(solution)/shard_map/ppermute | solution.py:392
  57.7 0.1 collective-permute-start.5
  57.8 0.5 collective-permute-start.6
  58.3 0.1 collective-permute-start.7
  58.4 2.2 %copy-done.4 = bf16[2048,1024]{1,0:T(8,128)(2,1)S(1)} copy-done((bf16[2048,1024]{1,0:T(8,128)(2,1)S(1)}, bf16[2048,1024]{1,0:T(8,128)(2,1)}, u32[]{:S(2)}) %copy-start.4) | copy-done | bytes 4194328
  60.6 2.2 %copy-done.10 = bf16[2048,1024]{1,0:T(8,128)(2,1)S(1)} copy-done((bf16[2048,1024]{1,0:T(8,128)(2,1)S(1)}, bf16[2048,1024]{1,0:T(8,128)(2,1)}, u32[]{:S(2)}) %copy-start.10) | copy-done | bytes 4194328
  62.7 3.5 %project.12 = bf16[256,512]{1,0:T(8,128)(2,1)S(1)} custom-call(s32[2]{0:T(128)S(1)} %pad_add_fusion.7.scalars, bf16[128,2048]{1,0:T(8,128)(2,1)S(1)} %collective-permute-done.9.mine, bf16[128,2048]{1,0:T(8,128)(2,1)S(1)} %collective-permute-done.10.other, bf16[2048,1024]{1,0:T(8,128)(2,1)S(1)} %copy-done.4, bf16[2048,1024]{1,0:T(8,128)(2,1)S(1)} %copy-done.10), custom_call_target="tpu_custom_call" | custom-call | flops 536870912 | bytes 2097152 | tf_op jit(solution)/shard_map/project/pallas_call | solution.py:79
  66.2 1.9 %collective-permute-start.11 = (bf16[256,512]{1,0:T(8,128)(2,1)S(1)}, bf16[256,512]{1,0:T(8,128)(2,1)}, u32[]{:S(2)}, u32[]{:S(2)}) collective-permute-start(bf16[256,512]{1,0:T(8,128)(2,1)S(1)} %project.12), channel_id=1, source_target_pairs={{16,16},{17,24},{18,17},{19,25},{20,18},{21,26},{22,19},{23,27},{2... | collective-permute-start | bytes 786440 | tf_op jit(solution)/shard_map/ppermute | solution.py:392
  68.2 3.5 %project.13 = bf16[256,512]{1,0:T(8,128)(2,1)S(1)} custom-call(s32[2]{0:T(128)S(1)} %pad_add_fusion.2.scalars, bf16[128,2048]{1,0:T(8,128)(2,1)S(1)} %collective-permute-done.9.mine, bf16[128,2048]{1,0:T(8,128)(2,1)S(1)} %collective-permute-done.10.other, bf16[2048,1024]{1,0:T(8,128)(2,1)S(1)} %copy-done.5, bf16[2048,1024]{1,0:T(8,128)(2,1)S(1)} %copy-done.11), custom_call_target="tpu_custom_call" | custom-call | flops 536870912 | bytes 2097152 | tf_op jit(solution)/shard_map/project/pallas_call | solution.py:79
  71.7 3.5 %project.14 = bf16[256,512]{1,0:T(8,128)(2,1)S(1)} custom-call(s32[2]{0:T(128)S(1)} %pad_add_fusion.3.scalars, bf16[128,2048]{1,0:T(8,128)(2,1)S(1)} %collective-permute-done.9.mine, bf16[128,2048]{1,0:T(8,128)(2,1)S(1)} %collective-permute-done.10.other, bf16[2048,1024]{1,0:T(8,128)(2,1)S(1)} %copy-done.5, bf16[2048,1024]{1,0:T(8,128)(2,1)S(1)} %copy-done.11), custom_call_target="tpu_custom_call" | custom-call | flops 536870912 | bytes 2097152 | tf_op jit(solution)/shard_map/project/pallas_call | solution.py:79
  75.1 3.5 %project.15 = bf16[256,512]{1,0:T(8,128)(2,1)S(1)} custom-call(s32[2]{0:T(128)S(1)} %pad_add_fusion.4.scalars, bf16[128,2048]{1,0:T(8,128)(2,1)S(1)} %collective-permute-done.9.mine, bf16[128,2048]{1,0:T(8,128)(2,1)S(1)} %collective-permute-done.10.other, bf16[2048,1024]{1,0:T(8,128)(2,1)S(1)} %copy-done.5, bf16[2048,1024]{1,0:T(8,128)(2,1)S(1)} %copy-done.11), custom_call_target="tpu_custom_call" | custom-call | flops 536870912 | bytes 2097152 | tf_op jit(solution)/shard_map/project/pallas_call | solution.py:79
  78.6 0.0 copy-start.21
  78.6 0.0 copy-start.22
  78.7 4.5 %collective-permute-start.12 = (bf16[256,512]{1,0:T(8,128)(2,1)S(1)}, bf16[256,512]{1,0:T(8,128)(2,1)S(1)}, u32[]{:S(2)}, u32[]{:S(2)}) collective-permute-start(bf16[256,512]{1,0:T(8,128)(2,1)S(1)} %project.13), channel_id=1, source_target_pairs={{16,18},{17,26},{18,19},{19,27},{20,16},{21,24},{22,17},{23,25},{2... | collective-permute-start | bytes 786440 | tf_op jit(solution)/shard_map/ppermute | solution.py:392
  83.2 3.0 %collective-permute-start.13 = (bf16[256,512]{1,0:T(8,128)(2,1)S(1)}, bf16[256,512]{1,0:T(8,128)(2,1)S(1)}, u32[]{:S(2)}, u32[]{:S(2)}) collective-permute-start(bf16[256,512]{1,0:T(8,128)(2,1)S(1)} %project.14), channel_id=1, source_target_pairs={{16,20},{17,28},{18,21},{19,29},{20,22},{21,30},{22,23},{23,31},{2... | collective-permute-start | bytes 786440 | tf_op jit(solution)/shard_map/ppermute | solution.py:392
  86.3 3.4 %collective-permute-start.14 = (bf16[256,512]{1,0:T(8,128)(2,1)S(1)}, bf16[256,512]{1,0:T(8,128)(2,1)S(1)}, u32[]{:S(2)}, u32[]{:S(2)}) collective-permute-start(bf16[256,512]{1,0:T(8,128)(2,1)S(1)} %project.15), channel_id=1, source_target_pairs={{16,22},{17,30},{18,23},{19,31},{20,20},{21,28},{22,21},{23,29},{2... | collective-permute-start | bytes 786440 | tf_op jit(solution)/shard_map/ppermute | solution.py:392
  89.7 0.1 pad_add_fusion.6.scalars
  89.7 0.1 pad_add_fusion.1.scalars
  89.8 0.1 pad_add_fusion.scalars
  89.9 0.0 collective-permute-start.8
  89.9 0.5 collective-permute-start.15
  90.4 0.1 collective-permute-start.16
  90.5 3.2 %collective-permute-done.13.refs_2_ = bf16[256,512]{1,0:T(8,128)(2,1)S(1)} collective-permute-done((bf16[256,512]{1,0:T(8,128)(2,1)S(1)}, bf16[256,512]{1,0:T(8,128)(2,1)S(1)}, u32[]{:S(2)}, u32[]{:S(2)}) %collective-permute-start.13) | collective-permute-done | bytes 262176 | tf_op jit(solution)/shard_map/ppermute | solution.py:392
  93.7 4.0 %collective-permute-done.14.refs_3_ = bf16[256,512]{1,0:T(8,128)(2,1)S(1)} collective-permute-done((bf16[256,512]{1,0:T(8,128)(2,1)S(1)}, bf16[256,512]{1,0:T(8,128)(2,1)S(1)}, u32[]{:S(2)}, u32[]{:S(2)}) %collective-permute-start.14) | collective-permute-done | bytes 262176 | tf_op jit(solution)/shard_map/ppermute | solution.py:392
  97.7 0.1 collective-permute-start.23
  97.8 7.0 %attend_own.1 = (bf16[1024,256]{1,0:T(8,128)(2,1)S(1)}, f32[2,1024,128]{2,1,0:T(8,128)S(1)}, f32[2,1024,256]{2,1,0:T(8,128)S(1)}) custom-call(s32[2]{0:T(128)S(1)} %pad_add_fusion.1.scalars, bf16[256,768]{1,0:T(8,128)(2,1)} %collective-permute-done.1.refs_0_, bf16[256,768]{1,0:T(8,128)(2,1)} %collective-permute-done.2.refs_1_, ...), custom_call_target="tpu_custom_call" | custom-call | flops 2147483648 | bytes 4194304 | tf_op jit(solution)/shard_map/attend_own/pallas_call | solution.py:207
  104.8 1.3 copy-done.23
  106.2 0.0 copy-start.18
  106.3 10.9 %attend_cross.1 = (bf16[256,256]{1,0:T(8,128)(2,1)S(1)}, bf16[256,256]{1,0:T(8,128)(2,1)S(1)}, bf16[256,256]{1,0:T(8,128)(2,1)S(1)}, bf16[256,256]{1,0:T(8,128)(2,1)S(1)}) custom-call(s32[3]{0:T(128)S(1)} %pad_add_fusion.scalars, f32[8]{0:T(128)S(1)} %copy-done.22, f32[1,256]{1,0:T(1,128)S(1)} %bitcast.12, bf16[1024,256]{1,0:T(8,128)(2,1)S(1)} %get-tuple-element.12.q_in, ...), custom_call_target="tpu_custom_call" | custom-call | flops 3221225472 | bytes 2097152 | tf_op jit(solution)/shard_map/attend_cross/pallas_call | solution.py:300
  117.2 4.8 %collective-permute-start.19 = (bf16[256,256]{1,0:T(8,128)(2,1)S(1)}, bf16[256,256]{1,0:T(8,128)(2,1)S(1)}, u32[]{:S(2)}, u32[]{:S(2)}) collective-permute-start(bf16[256,256]{1,0:T(8,128)(2,1)S(1)} %get-tuple-element.15), channel_id=1, source_target_pairs={{0,0},{8,1},{1,2},{9,3},{2,4},{10,5},{3,6},{11,7},{4,8},{12,9},{5,... | collective-permute-start | bytes 393224 | tf_op jit(solution)/shard_map/ppermute | solution.py:392
  122.0 1.5 %collective-permute-start.20 = (bf16[256,256]{1,0:T(8,128)(2,1)S(1)}, bf16[256,256]{1,0:T(8,128)(2,1)S(1)}, u32[]{:S(2)}, u32[]{:S(2)}) collective-permute-start(bf16[256,256]{1,0:T(8,128)(2,1)S(1)} %get-tuple-element.16), channel_id=1, source_target_pairs={{2,0},{10,1},{3,2},{11,3},{0,4},{8,5},{1,6},{9,7},{6,8},{14,9},{7,... | collective-permute-start | bytes 393224 | tf_op jit(solution)/shard_map/ppermute | solution.py:392
  123.6 1.2 collective-permute-start.21
  124.7 3.2 %collective-permute-start.22 = (bf16[256,256]{1,0:T(8,128)(2,1)S(1)}, bf16[256,256]{1,0:T(8,128)(2,1)S(1)}, u32[]{:S(2)}, u32[]{:S(2)}) collective-permute-start(bf16[256,256]{1,0:T(8,128)(2,1)S(1)} %get-tuple-element.18), channel_id=1, source_target_pairs={{6,0},{14,1},{7,2},{15,3},{4,4},{12,5},{5,6},{13,7},{2,8},{10,9},{... | collective-permute-start | bytes 393224 | tf_op jit(solution)/shard_map/ppermute | solution.py:392
  127.9 0.1 pad_add_fusion.5.scalars
  128.0 2.5 %pool.1.refs_5_ = f32[256,2048]{1,0:T(8,128)S(1)} custom-call(s32[3]{0:T(128)S(1)} %pad_add_fusion.5.scalars, bf16[128,2048]{1,0:T(8,128)(2,1)S(1)} %copy-done.17, bf16[128,2048]{1,0:T(8,128)(2,1)S(1)} %collective-permute-done.other, bf16[16,2048]{1,0:T(8,128)(2,1)S(1)} %collective-permute-done.23.rim, bf16[2048,512]{1,0:T(8,128)(2,1)S(1)} %copy-done.18, ...), custom_call_target="tpu_custom_call" | custom-call | flops 1073741824 | bytes 8388608 | tf_op jit(solution)/shard_map/pool/pallas_call | solution.py:125
  130.6 2.5 %collective-permute-done.22.refs_3_ = bf16[256,256]{1,0:T(8,128)(2,1)S(1)} collective-permute-done((bf16[256,256]{1,0:T(8,128)(2,1)S(1)}, bf16[256,256]{1,0:T(8,128)(2,1)S(1)}, u32[]{:S(2)}, u32[]{:S(2)}) %collective-permute-start.22) | collective-permute-done | bytes 131104 | tf_op jit(solution)/shard_map/ppermute | solution.py:392
  133.0 2.3 %output.3 = bf16[128,2048]{1,0:T(8,128)(2,1)S(1)} custom-call(s32[2]{0:T(128)S(1)} %pad_add_fusion.6.scalars, bf16[256,256]{1,0:T(8,128)(2,1)S(1)} %collective-permute-done.19.refs_0_, bf16[256,256]{1,0:T(8,128)(2,1)S(1)} %collective-permute-done.20.refs_1_, bf16[256,256]{1,0:T(8,128)(2,1)S(1)} %collective-permute-done.21.refs_2_, ...), custom_call_target="tpu_custom_call" | custom-call | flops 536870912 | bytes 4194304 | tf_op jit(solution)/shard_map/output/pallas_call | solution.py:344
  135.3 0.1 collective-permute-start.24
  135.4 2.3 %output.2 = bf16[128,2048]{1,0:T(8,128)(2,1)S(1)} custom-call(s32[2]{0:T(128)S(1)} %pad_add_fusion.7.scalars, bf16[256,256]{1,0:T(8,128)(2,1)S(1)} %collective-permute-done.19.refs_0_, bf16[256,256]{1,0:T(8,128)(2,1)S(1)} %collective-permute-done.20.refs_1_, bf16[256,256]{1,0:T(8,128)(2,1)S(1)} %collective-permute-done.21.refs_2_, ...), custom_call_target="tpu_custom_call" | custom-call | flops 536870912 | bytes 4194304 | tf_op jit(solution)/shard_map/output/pallas_call | solution.py:344
  137.8 0.9 add_convert_fusion
  (57 shorter events, 0.1 us)
Async XLA Ops:
  0.0 2.4 %collective-permute-start = (bf16[128,2048]{1,0:T(8,128)(2,1)}, bf16[128,2048]{1,0:T(8,128)(2,1)S(1)}, u32[]{:S(2)}, u32[]{:S(2)}) collective-permute-start(bf16[128,2048]{1,0:T(8,128)(2,1)} %mine.9), channel_id=1, source_target_pairs={{0,1},{1,0},{2,3},{3,2},{4,5},{5,4},{6,7},{7,6},{8,9},{9,8},{10,11... | collective-permute-start | bytes 1572872 | tf_op jit(solution)/shard_map/ppermute | solution.py:397
  0.7 24.3 %collective-permute-start.9 = (bf16[128,2048]{1,0:T(8,128)(2,1)}, bf16[128,2048]{1,0:T(8,128)(2,1)S(1)}, u32[]{:S(2)}, u32[]{:S(2)}) collective-permute-start(bf16[128,2048]{1,0:T(8,128)(2,1)} %mine.9), channel_id=1, source_target_pairs={{0,16},{2,18},{4,20},{6,22},{8,24},{10,26},{12,28},{14,30},{1,17},... | collective-permute-start | bytes 1572872 | tf_op jit(solution)/shard_map/ppermute | solution.py:414
  2.4 2.2 %copy-start = (bf16[2048,1024]{1,0:T(8,128)(2,1)S(1)}, bf16[2048,1024]{1,0:T(8,128)(2,1)}, u32[]{:S(2)}) copy-start(bf16[2048,1024]{1,0:T(8,128)(2,1)} %rest_0_.15) | copy-start | bytes 12582916
  4.6 2.2 %copy-start.6 = (bf16[2048,1024]{1,0:T(8,128)(2,1)S(1)}, bf16[2048,1024]{1,0:T(8,128)(2,1)}, u32[]{:S(2)}) copy-start(bf16[2048,1024]{1,0:T(8,128)(2,1)} %rest_1_.15) | copy-start | bytes 12582916
  6.8 2.2 %copy-start.12 = (bf16[2048,1024]{1,0:T(8,128)(2,1)S(1)}, bf16[2048,1024]{1,0:T(8,128)(2,1)}, u32[]{:S(2)}) copy-start(bf16[2048,1024]{1,0:T(8,128)(2,1)} %rest_0_.11) | copy-start | bytes 12582916
  9.0 1.0 copy-start.16
  10.0 8.2 %copy-start.1 = (bf16[2048,1024]{1,0:T(8,128)(2,1)S(1)}, bf16[2048,1024]{1,0:T(8,128)(2,1)}, u32[]{:S(2)}) copy-start(bf16[2048,1024]{1,0:T(8,128)(2,1)} %rest_0_.15) | copy-start | bytes 12582916
  10.0 8.2 %copy-start.7 = (bf16[2048,1024]{1,0:T(8,128)(2,1)S(1)}, bf16[2048,1024]{1,0:T(8,128)(2,1)}, u32[]{:S(2)}) copy-start(bf16[2048,1024]{1,0:T(8,128)(2,1)} %rest_1_.15) | copy-start | bytes 12582916
  10.0 8.2 %copy-start.17 = (bf16[128,2048]{1,0:T(8,128)(2,1)S(1)}, bf16[128,2048]{1,0:T(8,128)(2,1)}, u32[]{:S(2)}) copy-start(bf16[128,2048]{1,0:T(8,128)(2,1)} %mine.9) | copy-start | bytes 1572868
  14.7 43.0 %collective-permute-start.1 = (bf16[256,768]{1,0:T(8,128)(2,1)S(1)}, bf16[256,768]{1,0:T(8,128)(2,1)}, u32[]{:S(2)}, u32[]{:S(2)}) collective-permute-start(bf16[256,768]{1,0:T(8,128)(2,1)S(1)} %project.8), channel_id=1, source_target_pairs={{0,0},{1,8},{2,1},{3,9},{4,2},{5,10},{6,3},{7,11},{8,4},{9,12},{10... | collective-permute-start | bytes 1179656 | tf_op jit(solution)/shard_map/ppermute | solution.py:392
  22.9 34.9 %collective-permute-start.2 = (bf16[256,768]{1,0:T(8,128)(2,1)S(1)}, bf16[256,768]{1,0:T(8,128)(2,1)}, u32[]{:S(2)}, u32[]{:S(2)}) collective-permute-start(bf16[256,768]{1,0:T(8,128)(2,1)S(1)} %project.9), channel_id=1, source_target_pairs={{0,2},{1,10},{2,3},{3,11},{4,0},{5,8},{6,1},{7,9},{8,6},{9,14},{10... | collective-permute-start | bytes 1179656 | tf_op jit(solution)/shard_map/ppermute | solution.py:392
  25.0 33.4 %collective-permute-start.10 = (bf16[128,2048]{1,0:T(8,128)(2,1)S(1)}, bf16[128,2048]{1,0:T(8,128)(2,1)S(1)}, u32[]{:S(2)}, u32[]{:S(2)}) collective-permute-start(bf16[128,2048]{1,0:T(8,128)(2,1)S(1)} %collective-permute-done.9.mine), channel_id=1, source_target_pairs={{0,1},{1,0},{2,3},{3,2},{4,5},{5,4},{6,7},{7,6},{8,9},{9,8},{10,11... | collective-permute-start | bytes 1572872 | tf_op jit(solution)/shard_map/ppermute | solution.py:397
  25.1 2.2 %copy-start.2 = (bf16[2048,1024]{1,0:T(8,128)(2,1)S(1)}, bf16[2048,1024]{1,0:T(8,128)(2,1)}, u32[]{:S(2)}) copy-start(bf16[2048,1024]{1,0:T(8,128)(2,1)} %rest_0_.15) | copy-start | bytes 12582916
  27.3 2.2 %copy-start.8 = (bf16[2048,1024]{1,0:T(8,128)(2,1)S(1)}, bf16[2048,1024]{1,0:T(8,128)(2,1)}, u32[]{:S(2)}) copy-start(bf16[2048,1024]{1,0:T(8,128)(2,1)} %rest_1_.15) | copy-start | bytes 12582916
  29.5 2.2 %copy-start.13 = (bf16[2048,1024]{1,0:T(8,128)(2,1)S(1)}, bf16[2048,1024]{1,0:T(8,128)(2,1)}, u32[]{:S(2)}) copy-start(bf16[2048,1024]{1,0:T(8,128)(2,1)} %rest_0_.11) | copy-start | bytes 12582916
  37.0 21.2 %collective-permute-start.3 = (bf16[256,768]{1,0:T(8,128)(2,1)}, bf16[256,768]{1,0:T(8,128)(2,1)}, u32[]{:S(2)}, u32[]{:S(2)}) collective-permute-start(bf16[256,768]{1,0:T(8,128)(2,1)} %project.10), channel_id=1, source_target_pairs={{0,4},{1,12},{2,5},{3,13},{4,6},{5,14},{6,7},{7,15},{8,0},{9,8},{1... | collective-permute-start | bytes 1179656 | tf_op jit(solution)/shard_map/ppermute | solution.py:392
  43.5 2.2 %copy-start.3 = (bf16[2048,1024]{1,0:T(8,128)(2,1)S(1)}, bf16[2048,1024]{1,0:T(8,128)(2,1)}, u32[]{:S(2)}) copy-start(bf16[2048,1024]{1,0:T(8,128)(2,1)} %rest_0_.15) | copy-start | bytes 12582916
  45.7 2.2 %copy-start.9 = (bf16[2048,1024]{1,0:T(8,128)(2,1)S(1)}, bf16[2048,1024]{1,0:T(8,128)(2,1)}, u32[]{:S(2)}) copy-start(bf16[2048,1024]{1,0:T(8,128)(2,1)} %rest_1_.15) | copy-start | bytes 12582916
  47.9 2.2 %copy-start.14 = (bf16[2048,1024]{1,0:T(8,128)(2,1)S(1)}, bf16[2048,1024]{1,0:T(8,128)(2,1)}, u32[]{:S(2)}) copy-start(bf16[2048,1024]{1,0:T(8,128)(2,1)} %rest_0_.11) | copy-start | bytes 12582916
  54.7 23.9 %collective-permute-start.4 = (bf16[256,768]{1,0:T(8,128)(2,1)S(1)}, bf16[256,768]{1,0:T(8,128)(2,1)}, u32[]{:S(2)}, u32[]{:S(2)}) collective-permute-start(bf16[256,768]{1,0:T(8,128)(2,1)S(1)} %project.11), channel_id=1, source_target_pairs={{0,6},{1,14},{2,7},{3,15},{4,4},{5,12},{6,5},{7,13},{8,2},{9,10},{... | collective-permute-start | bytes 1179656 | tf_op jit(solution)/shard_map/ppermute | solution.py:392
  57.7 25.5 %collective-permute-start.5 = (bf16[256,768]{1,0:T(8,128)(2,1)}, bf16[256,768]{1,0:T(8,128)(2,1)}, u32[]{:S(2)}, u32[]{:S(2)}) collective-permute-start(bf16[256,768]{1,0:T(8,128)(2,1)} %collective-permute-done.1.refs_0_), channel_id=1, source_target_pairs={{0,1},{1,0},{2,3},{3,2},{4,5},{5,4},{6,7},{7,6},{8,9},{9,8},{10,11... | collective-permute-start | bytes 1179656 | tf_op jit(solution)/shard_map/ppermute | solution.py:397
  57.8 28.5 %collective-permute-start.6 = (bf16[256,768]{1,0:T(8,128)(2,1)}, bf16[256,768]{1,0:T(8,128)(2,1)}, u32[]{:S(2)}, u32[]{:S(2)}) collective-permute-start(bf16[256,768]{1,0:T(8,128)(2,1)} %collective-permute-done.2.refs_1_), channel_id=1, source_target_pairs={{0,1},{1,0},{2,3},{3,2},{4,5},{5,4},{6,7},{7,6},{8,9},{9,8},{10,11... | collective-permute-start | bytes 1179656 | tf_op jit(solution)/shard_map/ppermute | solution.py:397
  58.3 31.6 %collective-permute-start.7 = (bf16[256,768]{1,0:T(8,128)(2,1)}, bf16[256,768]{1,0:T(8,128)(2,1)}, u32[]{:S(2)}, u32[]{:S(2)}) collective-permute-start(bf16[256,768]{1,0:T(8,128)(2,1)} %collective-permute-done.3.refs_2_), channel_id=1, source_target_pairs={{0,1},{1,0},{2,3},{3,2},{4,5},{5,4},{6,7},{7,6},{8,9},{9,8},{10,11... | collective-permute-start | bytes 1179656 | tf_op jit(solution)/shard_map/ppermute | solution.py:397
  58.4 2.2 %copy-start.4 = (bf16[2048,1024]{1,0:T(8,128)(2,1)S(1)}, bf16[2048,1024]{1,0:T(8,128)(2,1)}, u32[]{:S(2)}) copy-start(bf16[2048,1024]{1,0:T(8,128)(2,1)} %rest_0_.15) | copy-start | bytes 12582916
  60.6 2.2 %copy-start.10 = (bf16[2048,1024]{1,0:T(8,128)(2,1)S(1)}, bf16[2048,1024]{1,0:T(8,128)(2,1)}, u32[]{:S(2)}) copy-start(bf16[2048,1024]{1,0:T(8,128)(2,1)} %rest_1_.15) | copy-start | bytes 12582916
  62.7 5.4 %copy-start.5 = (bf16[2048,1024]{1,0:T(8,128)(2,1)S(1)}, bf16[2048,1024]{1,0:T(8,128)(2,1)}, u32[]{:S(2)}) copy-start(bf16[2048,1024]{1,0:T(8,128)(2,1)} %rest_0_.15) | copy-start | bytes 12582916
  62.7 5.4 %copy-start.11 = (bf16[2048,1024]{1,0:T(8,128)(2,1)S(1)}, bf16[2048,1024]{1,0:T(8,128)(2,1)}, u32[]{:S(2)}) copy-start(bf16[2048,1024]{1,0:T(8,128)(2,1)} %rest_1_.15) | copy-start | bytes 12582916
  66.2 23.7 %collective-permute-start.11 = (bf16[256,512]{1,0:T(8,128)(2,1)S(1)}, bf16[256,512]{1,0:T(8,128)(2,1)}, u32[]{:S(2)}, u32[]{:S(2)}) collective-permute-start(bf16[256,512]{1,0:T(8,128)(2,1)S(1)} %project.12), channel_id=1, source_target_pairs={{16,16},{17,24},{18,17},{19,25},{20,18},{21,26},{22,19},{23,27},{2... | collective-permute-start | bytes 786440 | tf_op jit(solution)/shard_map/ppermute | solution.py:392
  78.6 27.6 %copy-start.21 = (f32[256]{0:T(256)S(1)}, f32[256]{0:T(256)}, u32[]{:S(2)}) copy-start(f32[256]{0:T(256)} %param.17) | copy-start | bytes 3076
  78.6 27.6 %copy-start.22 = (f32[8]{0:T(128)S(1)}, f32[8]{0:T(128)}, u32[]{:S(2)}) copy-start(f32[8]{0:T(128)} %balance.1) | copy-start | bytes 100
  78.7 11.8 %collective-permute-start.12 = (bf16[256,512]{1,0:T(8,128)(2,1)S(1)}, bf16[256,512]{1,0:T(8,128)(2,1)S(1)}, u32[]{:S(2)}, u32[]{:S(2)}) collective-permute-start(bf16[256,512]{1,0:T(8,128)(2,1)S(1)} %project.13), channel_id=1, source_target_pairs={{16,18},{17,26},{18,19},{19,27},{20,16},{21,24},{22,17},{23,25},{2... | collective-permute-start | bytes 786440 | tf_op jit(solution)/shard_map/ppermute | solution.py:392
  83.2 10.5 %collective-permute-start.13 = (bf16[256,512]{1,0:T(8,128)(2,1)S(1)}, bf16[256,512]{1,0:T(8,128)(2,1)S(1)}, u32[]{:S(2)}, u32[]{:S(2)}) collective-permute-start(bf16[256,512]{1,0:T(8,128)(2,1)S(1)} %project.14), channel_id=1, source_target_pairs={{16,20},{17,28},{18,21},{19,29},{20,22},{21,30},{22,23},{23,31},{2... | collective-permute-start | bytes 786440 | tf_op jit(solution)/shard_map/ppermute | solution.py:392
  86.3 11.4 %collective-permute-start.14 = (bf16[256,512]{1,0:T(8,128)(2,1)S(1)}, bf16[256,512]{1,0:T(8,128)(2,1)S(1)}, u32[]{:S(2)}, u32[]{:S(2)}) collective-permute-start(bf16[256,512]{1,0:T(8,128)(2,1)S(1)} %project.15), channel_id=1, source_target_pairs={{16,22},{17,30},{18,23},{19,31},{20,20},{21,28},{22,21},{23,29},{2... | collective-permute-start | bytes 786440 | tf_op jit(solution)/shard_map/ppermute | solution.py:392
  89.9 7.8 %collective-permute-start.8 = (bf16[256,768]{1,0:T(8,128)(2,1)}, bf16[256,768]{1,0:T(8,128)(2,1)S(1)}, u32[]{:S(2)}, u32[]{:S(2)}) collective-permute-start(bf16[256,768]{1,0:T(8,128)(2,1)} %collective-permute-done.4.refs_3_), channel_id=1, source_target_pairs={{0,1},{1,0},{2,3},{3,2},{4,5},{5,4},{6,7},{7,6},{8,9},{9,8},{10,11... | collective-permute-start | bytes 1179656 | tf_op jit(solution)/shard_map/ppermute | solution.py:397
  89.9 16.2 %collective-permute-start.15 = (bf16[256,512]{1,0:T(8,128)(2,1)}, bf16[256,512]{1,0:T(8,128)(2,1)S(1)}, u32[]{:S(2)}, u32[]{:S(2)}) collective-permute-start(bf16[256,512]{1,0:T(8,128)(2,1)} %collective-permute-done.11.refs_0_), channel_id=1, source_target_pairs={{0,1},{1,0},{2,3},{3,2},{4,5},{5,4},{6,7},{7,6},{8,9},{9,8},{10,11... | collective-permute-start | bytes 786440 | tf_op jit(solution)/shard_map/ppermute | solution.py:397
  90.4 15.8 %collective-permute-start.16 = (bf16[256,512]{1,0:T(8,128)(2,1)S(1)}, bf16[256,512]{1,0:T(8,128)(2,1)S(1)}, u32[]{:S(2)}, u32[]{:S(2)}) collective-permute-start(bf16[256,512]{1,0:T(8,128)(2,1)S(1)} %collective-permute-done.12.refs_1_), channel_id=1, source_target_pairs={{0,1},{1,0},{2,3},{3,2},{4,5},{5,4},{6,7},{7,6},{8,9},{9,8},{10,11... | collective-permute-start | bytes 786440 | tf_op jit(solution)/shard_map/ppermute | solution.py:397
  93.7 12.5 %collective-permute-start.17 = (bf16[256,512]{1,0:T(8,128)(2,1)S(1)}, bf16[256,512]{1,0:T(8,128)(2,1)S(1)}, u32[]{:S(2)}, u32[]{:S(2)}) collective-permute-start(bf16[256,512]{1,0:T(8,128)(2,1)S(1)} %collective-permute-done.13.refs_2_), channel_id=1, source_target_pairs={{0,1},{1,0},{2,3},{3,2},{4,5},{5,4},{6,7},{7,6},{8,9},{9,8},{10,11... | collective-permute-start | bytes 786440 | tf_op jit(solution)/shard_map/ppermute | solution.py:397
  97.7 8.5 %collective-permute-start.18 = (bf16[256,512]{1,0:T(8,128)(2,1)S(1)}, bf16[256,512]{1,0:T(8,128)(2,1)S(1)}, u32[]{:S(2)}, u32[]{:S(2)}) collective-permute-start(bf16[256,512]{1,0:T(8,128)(2,1)S(1)} %collective-permute-done.14.refs_3_), channel_id=1, source_target_pairs={{0,1},{1,0},{2,3},{3,2},{4,5},{5,4},{6,7},{7,6},{8,9},{9,8},{10,11... | collective-permute-start | bytes 786440 | tf_op jit(solution)/shard_map/ppermute | solution.py:397
  97.7 30.3 %collective-permute-start.23 = (bf16[16,2048]{1,0:T(8,128)(2,1)S(1)}, bf16[16,2048]{1,0:T(8,128)(2,1)S(1)}, u32[]{:S(2)}, u32[]{:S(2)}) collective-permute-start(bf16[16,2048]{1,0:T(8,128)(2,1)S(1)} %slice_select_fusion), channel_id=1, source_target_pairs={{0,2},{2,4},{4,6},{6,8},{8,10},{10,12},{12,14},{14,16},{16,18},{18... | collective-permute-start | bytes 196616 | tf_op jit(solution)/shard_map/ppermute | solution.py:433
  104.8 1.3 copy-start.23
  106.2 21.8 %copy-start.18 = (bf16[2048,512]{1,0:T(8,128)(2,1)S(1)}, bf16[2048,512]{1,0:T(8,128)(2,1)}, u32[]{:S(2)}) copy-start(bf16[2048,512]{1,0:T(8,128)(2,1)} %w_in.1) | copy-start | bytes 6291460
  106.2 21.8 %copy-start.19 = (bf16[512,2048]{1,0:T(8,128)(2,1)S(1)}, bf16[512,2048]{1,0:T(8,128)(2,1)}, u32[]{:S(2)}) copy-start(bf16[512,2048]{1,0:T(8,128)(2,1)} %w_out.1) | copy-start | bytes 6291460
  106.2 21.8 %copy-start.20 = (bf16[4,128,128]{2,1,0:T(8,128)(2,1)S(1)}, bf16[4,128,128]{2,1,0:T(8,128)(2,1)}, u32[]{:S(2)}) copy-start(bf16[4,128,128]{2,1,0:T(8,128)(2,1)} %w_mix.1) | copy-start | bytes 393220
  117.2 15.8 %copy-start.15 = (bf16[1024,2048]{1,0:T(8,128)(2,1)S(1)}, bf16[1024,2048]{1,0:T(8,128)(2,1)}, u32[]{:S(2)}) copy-start(bf16[1024,2048]{1,0:T(8,128)(2,1)} %refs_4_.3) | copy-start | bytes 12582916
  117.2 13.3 %collective-permute-start.19 = (bf16[256,256]{1,0:T(8,128)(2,1)S(1)}, bf16[256,256]{1,0:T(8,128)(2,1)S(1)}, u32[]{:S(2)}, u32[]{:S(2)}) collective-permute-start(bf16[256,256]{1,0:T(8,128)(2,1)S(1)} %get-tuple-element.15), channel_id=1, source_target_pairs={{0,0},{8,1},{1,2},{9,3},{2,4},{10,5},{3,6},{11,7},{4,8},{12,9},{5,... | collective-permute-start | bytes 393224 | tf_op jit(solution)/shard_map/ppermute | solution.py:392
  122.0 8.5 %collective-permute-start.20 = (bf16[256,256]{1,0:T(8,128)(2,1)S(1)}, bf16[256,256]{1,0:T(8,128)(2,1)S(1)}, u32[]{:S(2)}, u32[]{:S(2)}) collective-permute-start(bf16[256,256]{1,0:T(8,128)(2,1)S(1)} %get-tuple-element.16), channel_id=1, source_target_pairs={{2,0},{10,1},{3,2},{11,3},{0,4},{8,5},{1,6},{9,7},{6,8},{14,9},{7,... | collective-permute-start | bytes 393224 | tf_op jit(solution)/shard_map/ppermute | solution.py:392
  123.6 7.0 %collective-permute-start.21 = (bf16[256,256]{1,0:T(8,128)(2,1)S(1)}, bf16[256,256]{1,0:T(8,128)(2,1)S(1)}, u32[]{:S(2)}, u32[]{:S(2)}) collective-permute-start(bf16[256,256]{1,0:T(8,128)(2,1)S(1)} %get-tuple-element.17), channel_id=1, source_target_pairs={{4,0},{12,1},{5,2},{13,3},{6,4},{14,5},{7,6},{15,7},{0,8},{8,9},{1... | collective-permute-start | bytes 393224 | tf_op jit(solution)/shard_map/ppermute | solution.py:392
  124.7 8.3 %collective-permute-start.22 = (bf16[256,256]{1,0:T(8,128)(2,1)S(1)}, bf16[256,256]{1,0:T(8,128)(2,1)S(1)}, u32[]{:S(2)}, u32[]{:S(2)}) collective-permute-start(bf16[256,256]{1,0:T(8,128)(2,1)S(1)} %get-tuple-element.18), channel_id=1, source_target_pairs={{6,0},{14,1},{7,2},{15,3},{4,4},{12,5},{5,6},{13,7},{2,8},{10,9},{... | collective-permute-start | bytes 393224 | tf_op jit(solution)/shard_map/ppermute | solution.py:392
  135.3 2.4 %collective-permute-start.24 = (bf16[128,2048]{1,0:T(8,128)(2,1)S(1)}, bf16[128,2048]{1,0:T(8,128)(2,1)S(1)}, u32[]{:S(2)}, u32[]{:S(2)}) collective-permute-start(bf16[128,2048]{1,0:T(8,128)(2,1)S(1)} %output.3), channel_id=1, source_target_pairs={{0,1},{1,0},{2,3},{3,2},{4,5},{5,4},{6,7},{7,6},{8,9},{9,8},{10,11... | collective-permute-start | bytes 1572872 | tf_op jit(solution)/shard_map/ppermute | solution.py:397
